TPU v7x, 128 devices: a whole 4x4x4 slice. The times are simulated.
128 devices in a mesh: fs: 16 (over z, x), tp: 8 (over y, core).
Axes of the slice: x: 4, y: 4, z: 4, core: 2. Of those that a mesh axis runs over, the one named last changes fastest.
Arguments:
- normed_input: bfloat16 [32768, 2048], P('fs'), may hold values from -6 to 6
- forget_cot: bfloat16 [32768, 2048], P('fs', 'tp'), may hold values from -6 to 6
- value_cot: bfloat16 [32768, 2048], P('fs', 'tp'), may hold values from -6 to 6
- gated_output: bfloat16 [32768, 2048], P('fs', 'tp'), may hold values from -6 to 6
- output_cot: bfloat16 [32768, 2048], P('fs'), may hold values from -6 to 6
- forget_weight: float32 [2048, 2048], P('fs', 'tp'), may hold values from -0.125 to 0.125
- value_weight: float32 [2048, 2048], P('fs', 'tp'), may hold values from -0.125 to 0.125
- out_weight: float32 [2048, 2048], P('tp', 'fs'), may hold values from -0.125 to 0.125
- bases: bfloat16 [3, 2048, 256], replicated, may hold values from -0.125 to 0.125
- first_moment: float32 [256, 3, 2048], P('fs', None, 'tp'), may hold values from -4 to 4
- second_moment: float32 [256, 3, 2048], P('fs', None, 'tp'), may hold values from 0.25 to 4
Outputs:
- new_forget: float32 [2048, 2048], P('fs', 'tp')
- new_value: float32 [2048, 2048], P('fs', 'tp')
- new_out: float32 [2048, 2048], P('tp', 'fs')
- copy_forget: bfloat16 [2048, 2048], P(None, 'tp')
- copy_value: bfloat16 [2048, 2048], P(None, 'tp')
- copy_out: bfloat16 [2048, 2048], P('tp')
- moment_one: float32 [256, 3, 2048], P('fs', None, 'tp')
- moment_two: float32 [256, 3, 2048], P('fs', None, 'tp')
- step_forget: float32 [2048, 2048], P('fs', 'tp')
- step_value: float32 [2048, 2048], P('fs', 'tp')
- step_out: float32 [2048, 2048], P('tp', 'fs')
All inputs are finite; a program needn't handle non-finite values.
Results may differ from a plain program's by a relative error of at most 0.0045.
Values may be sent and summed in bfloat16 or wider, within the bound.
No kernel may reach another device: no remote copies, remote signals or barrier semaphores. Data moves between devices by JAX's collectives and lax.ppermute only.
A program may use at most 128 MiB of HBM per device.

v0:
```python
import functools

import jax
import jax.numpy as jnp
from jax import lax
from jax.sharding import Mesh
from jax.sharding import PartitionSpec as P

FS = ("fs_0", "fs_1")
FS_TP = ("fs_0", "fs_1", "tp_0", "tp_1")
TP = ("tp_0", "tp_1")


def in_blocks(value, dim, count):
    before, after = (value.shape[:dim], value.shape[dim + 1 :])
    return jnp.moveaxis(value.reshape(*before, count, -1, *after), dim, 0)


def sum_at_owner(value, axis, dim):
    pieces = in_blocks(value, dim, lax.axis_size(axis))
    arrived = lax.all_to_all(pieces, axis, split_axis=0, concat_axis=0, tiled=True)
    return arrived.astype(jnp.float32).sum(axis=0)


def joined_along(pieces, dim):
    dims = list(pieces.shape[1:])
    dims[dim] *= pieces.shape[0]
    return jnp.moveaxis(pieces, 0, dim).reshape(dims)


def sent_to_all(value, axis):
    copies = jnp.broadcast_to(value, (lax.axis_size(axis), *value.shape))
    return lax.all_to_all(copies, axis, split_axis=0, concat_axis=0, tiled=True)


def gather_directly(value, axis, dim):
    return joined_along(sent_to_all(value, axis), dim)


def over_axes(value, axes):
    return functools.reduce(lax.psum, axes, value)


def gather_turned(arrays, axis, dims):
    turned = [jnp.moveaxis(a, dim, 0) for a, dim in zip(arrays, dims)]
    both = jnp.concatenate([t.reshape(len(t), -1) for t in turned], axis=1)
    result, at, finished = (lax.all_gather(both, axis, axis=0, tiled=True), 0, [])
    for t, dim in zip(turned, dims):
        piece = result[:, at : at + t[0].size].reshape(-1, *t.shape[1:])
        finished.append(jnp.moveaxis(piece, 0, dim))
        at += t[0].size
    return tuple(finished)


def split_parts(values):
    high = lax.optimization_barrier(values.astype(jnp.bfloat16))
    low = (values - high.astype(jnp.float32)).astype(jnp.bfloat16)
    return (high, low)


def on_device(
    normed_input,
    forget_cot,
    value_cot,
    gated_output,
    output_cot,
    forget_weight,
    value_weight,
    out_weight,
    bases,
    first_moment,
    second_moment,
):
    rows = forget_weight.shape[0]
    rank_rows = first_moment.shape[0]
    columns = forget_weight.shape[1]
    offset = lax.axis_index(FS) * rows
    factor = float(normed_input.shape[0] * lax.axis_size(FS)) ** (-0.5)
    my_bases = lax.dynamic_slice_in_dim(bases, offset, rows, 1)
    reduced = jnp.stack(
        [
            jnp.dot(normed_input, bases[0], preferred_element_type=jnp.float32),
            jnp.dot(normed_input, bases[1], preferred_element_type=jnp.float32),
            jnp.dot(output_cot, bases[2], preferred_element_type=jnp.float32),
        ],
        axis=1,
    )
    reduced_high, reduced_low = split_parts(reduced)
    paired = jnp.stack([forget_cot, value_cot, gated_output], axis=1)
    upper = jnp.einsum("tkr,tkc->rkc", reduced_high, paired, preferred_element_type=jnp.float32)
    lower = jnp.einsum("tkr,tkc->rkc", reduced_low, paired, preferred_element_type=jnp.float32)
    projected = sum_at_owner(((upper + lower) * factor).astype(jnp.bfloat16), FS, 0)
    moment_one = 0.9 * first_moment + 0.1 * projected
    moment_two = 0.9 * second_moment + 0.1 * projected * projected
    direction = moment_one / (jnp.sqrt(moment_two) + 1e-08)
    piece_high, piece_low = split_parts(gather_directly(direction, FS, 0))
    upper = jnp.einsum("kdr,rkc->dkc", my_bases, piece_high, preferred_element_type=jnp.float32)
    lower = jnp.einsum("kdr,rkc->dkc", my_bases, piece_low, preferred_element_type=jnp.float32)
    full = upper + lower
    totals = over_axes(jnp.sum(direction * direction, axis=(0, 2)), FS_TP)
    entries = rank_rows * lax.axis_size(FS) * columns * lax.axis_size(TP)
    scale = lax.rsqrt(totals / entries + 1.0)
    full = full * scale[None, :, None]
    step_forget = full[:, 0, :]
    step_value = full[:, 1, :]
    step_out = full[:, 2, :].T
    new_forget = forget_weight - 0.01 * step_forget
    new_value = value_weight - 0.01 * step_value
    new_out = out_weight - 0.01 * step_out
    copy_forget, copy_value, copy_out = gather_turned(
        (
            new_forget.astype(jnp.bfloat16),
            new_value.astype(jnp.bfloat16),
            new_out.astype(jnp.bfloat16),
        ),
        FS,
        (0, 0, 1),
    )
    return (
        new_forget,
        new_value,
        new_out,
        copy_forget,
        copy_value,
        copy_out,
        moment_one,
        moment_two,
        step_forget,
        step_value,
        step_out,
    )


def solution(mesh):
    torus = Mesh(mesh.devices.reshape(4, 4, 4, 2), ("fs_0", "fs_1", "tp_0", "tp_1"))
    placed = (
        P(FS, None),
        P(FS, TP),
        P(FS, TP),
        P(FS, TP),
        P(FS, None),
        P(FS, TP),
        P(FS, TP),
        P(TP, FS),
        P(),
        P(FS, None, TP),
        P(FS, None, TP),
    )
    return jax.shard_map(
        on_device,
        mesh=torus,
        in_specs=placed,
        out_specs=(
            P(FS, TP),
            P(FS, TP),
            P(TP, FS),
            P(None, TP),
            P(None, TP),
            P(TP, None),
            P(FS, None, TP),
            P(FS, None, TP),
            P(FS, TP),
            P(FS, TP),
            P(TP, FS),
        ),
        check_vma=False,
    )
```

profile of v0, /device:TPU:0, one launch (start us, length us, event | category | flops | bytes accessed | tf_op | source)
XLA Modules:
  0.0 149.7 jit_solution(3815490610961850263)
XLA Ops:
  7.2 0.0 copy-start.3
  7.2 0.0 slice-start
  7.2 6.1 %convolution_bitcast_fusion.1 = f32[2048,1,256]{2,0,1:T(8,128)S(1)} fusion(bf16[2048,2048]{1,0:T(8,128)(2,1)} %param.11, bf16[3,2048,256]{2,1,0:T(8,128)(2,1)} %param.19), kind=kOutput, calls=%fused_computation.6 | convolution fusion | flops 2147483648 | bytes 11534336 | tf_op jit(solution)/shard_map/dot_general | solution.py:83
  13.3 0.9 copy-done.6
  14.2 2.5 %convolution_bitcast_fusion.2 = f32[2048,1,256]{2,0,1:T(8,128)S(1)} fusion(bf16[2048,2048]{1,0:T(8,128)(2,1)S(1)} %copy-done.6, bf16[3,2048,256]{2,1,0:T(8,128)(2,1)S(1)} %copy-done.3), kind=kOutput, calls=%fused_computation.7 | convolution fusion | flops 2147483648 | bytes 11534336 | tf_op jit(solution)/shard_map/dot_general | solution.py:82
  16.7 0.1 slice-done.1
  16.8 2.4 %convolution_bitcast_fusion = f32[2048,1,256]{2,0,1:T(8,128)S(1)} fusion(bf16[2048,2048]{1,0:T(8,128)(2,1)S(1)} %bitcast.55, bf16[3,2048,256]{2,1,0:T(8,128)(2,1)S(1)} %copy-done.3), kind=kOutput, calls=%fused_computation.5 | convolution fusion | flops 2147483648 | bytes 11534336 | tf_op jit(solution)/shard_map/dot_general | solution.py:84
  19.2 0.0 copy-start.7
  19.2 0.0 copy-start.8
  19.2 0.0 copy-start.9
  19.2 0.6 fusion
  19.8 0.6 copy-done.7
  20.4 0.3 copy-done.8
  20.7 0.3 copy-done.9
  21.1 1.4 fusion.1
  22.5 0.0 copy-start.4
  22.5 0.0 copy-start.5
  22.5 1.3 fusion.5
  23.8 0.0 copy-start
  23.8 0.0 copy-start.1
  23.9 18.0 %all_to_all.10 = bf16[16,16,3,256]{3,1,2,0:T(8,128)(2,1)S(1)} all-to-all(bf16[16,16,3,256]{3,1,2,0:T(8,128)(2,1)S(1)} %copy.47), channel_id=1, replica_groups=mesh['fs_0'=4,'fs_1'=4,'tp_0'=4,'tp_1'=2] {'fs_0','fs_1'}, dimensions={0} | all-to-all | bytes 786432 | tf_op jit(solution)/shard_map/all_to_all | solution.py:21
  41.9 0.1 convert_reduce_fusion
  42.0 0.7 multiply_reduce_fusion
  42.6 1.0 broadcast_in_dim.4
  43.6 3.6 %all-to-all-start.1 = ((f32[16,16,3,256]{3,1,2,0:T(8,128)}), f32[16,16,3,256]{3,1,2,0:T(8,128)S(1)}, u32[]{:S(2)}, u32[]{:S(2)}) async-start(f32[16,16,3,256]{3,1,2,0:T(8,128)} %broadcast_in_dim.4), calls=%async_computation.1 | async-start | bytes 1572864 | tf_op jit(solution)/shard_map/all_to_all | solution.py:33
  47.2 0.0 all-gather.2.cloned.1.call-start
  47.3 14.0 %psum.28 = f32[3]{0:T(128)S(1)} all-reduce(f32[3]{0:T(128)S(1)} %get-tuple-element.51), channel_id=1, replica_groups=mesh['fs_0'=4,'fs_1'=4,'tp_0'=4,'tp_1'=2] {'fs_0'}, use_global_device_ids=true, to_apply=%region_2.0 | all-reduce | flops 3 | bytes 24 | tf_op jit(solution)/shard_map/psum | solution.py:41
  61.3 0.1 copy.51
  61.4 10.5 %psum.29 = f32[3]{0:T(128)S(1)} all-reduce(f32[3]{0:T(128)S(1)} %psum.28), channel_id=1, replica_groups=mesh['fs_0'=4,'fs_1'=4,'tp_0'=4,'tp_1'=2] {'fs_1'}, use_global_device_ids=true, to_apply=%region_3.0 | all-reduce | flops 3 | bytes 24 | tf_op jit(solution)/shard_map/psum | solution.py:41
  71.9 0.1 copy.52
  72.0 10.7 %psum.30 = f32[3]{0:T(128)S(1)} all-reduce(f32[3]{0:T(128)S(1)} %psum.29), channel_id=1, replica_groups=mesh['fs_0'=4,'fs_1'=4,'tp_0'=4,'tp_1'=2] {'tp_0'}, use_global_device_ids=true, to_apply=%region_4.0 | all-reduce | flops 3 | bytes 24 | tf_op jit(solution)/shard_map/psum | solution.py:41
  82.7 2.5 %psum.31 = f32[3]{0:T(128)S(1)} all-reduce(f32[3]{0:T(128)S(1)} %psum.30), channel_id=1, replica_groups=mesh['fs_0'=4,'fs_1'=4,'tp_0'=4,'tp_1'=2] {'tp_1'}, use_global_device_ids=true, to_apply=%region_5.0 | all-reduce | flops 3 | bytes 24 | tf_op jit(solution)/shard_map/psum | solution.py:41
  85.2 0.0 all-to-all-done.1
  85.2 0.1 copy.48
  85.3 0.1 fusion.14
  85.4 1.2 fusion.16
  86.7 1.2 fusion.7
  87.9 0.7 convert_bitcast_fusion
  88.7 0.7 pad_maximum_fusion.10
  89.4 0.0 all-gather.2.cloned.1.call-update
  89.4 0.8 copy.53
  90.2 0.8 copy.54
  91.0 0.8 copy.57
  91.7 0.8 copy.58
  92.5 44.7 %all-gather.2.cloned.1.call-done = bf16[2048,768]{0,1:T(8,128)(2,1)} async-done(((bf16[128,768]{0,1:T(8,128)(2,1)}), bf16[2048,768]{0,1:T(8,128)(2,1)}) %all-gather.2.cloned.1.call-update) | async-done | bytes 3145744 | tf_op jit(solution)/shard_map/all_gather | solution.py:47
  137.2 3.1 %slice_bitcast_fusion = (bf16[256,2048]{1,0:T(8,128)(2,1)}, bf16[2048,256]{0,1:T(8,128)(2,1)S(1)}, bf16[2048,256]{0,1:T(8,128)(2,1)S(1)}) fusion(bf16[2048,768]{0,1:T(8,128)(2,1)} %all-gather.2.cloned.1.call-done), kind=kLoop, calls=%fused_computation.15 | loop fusion | bytes 6291456 | tf_op jit(solution)/shard_map/transpose | solution.py:50
  140.3 1.3 copy.55
  141.6 1.3 copy.56
  (16 shorter events, 0.2 us)
Async XLA Ops:
  7.2 6.2 %copy-start.3 = (bf16[3,2048,256]{2,1,0:T(8,128)(2,1)S(1)}, bf16[3,2048,256]{2,1,0:T(8,128)(2,1)}, u32[]{:S(2)}) copy-start(bf16[3,2048,256]{2,1,0:T(8,128)(2,1)} %param.19) | copy-start | bytes 9437188
  7.2 7.0 %copy-start.6 = (bf16[2048,2048]{1,0:T(8,128)(2,1)S(1)}, bf16[2048,2048]{1,0:T(8,128)(2,1)}, u32[]{:S(2)}) copy-start(bf16[2048,2048]{1,0:T(8,128)(2,1)} %param.11) | copy-start | bytes 25165828
  7.2 9.5 %slice-start = ((s8[8388608]{0:T(1024)(128)(4,1)}), s8[4194304]{0:T(1024)(128)(4,1)S(1)}, s32[]{:S(2)}) async-start(s8[8388608]{0:T(1024)(128)(4,1)} %bitcast.54), calls=%async_computation.3 | async-start | bytes 8388608
  14.2 2.6 %slice-start.1 = ((s8[8388608]{0:T(1024)(128)(4,1)}), s8[4194304]{0:T(1024)(128)(4,1)S(1)}, s32[]{:S(2)}) async-start(s8[8388608]{0:T(1024)(128)(4,1)} %bitcast.54), calls=%async_computation.4 | async-start | bytes 8388608
  19.2 1.2 copy-start.7
  19.2 1.5 %copy-start.8 = (bf16[2048,256]{1,0:T(8,128)(2,1)S(1)}, bf16[2048,256]{1,0:T(8,128)(2,1)}, u32[]{:S(2)}) copy-start(bf16[2048,256]{1,0:T(8,128)(2,1)} %param.13) | copy-start | bytes 3145732
  19.2 1.8 %copy-start.9 = (bf16[2048,256]{1,0:T(8,128)(2,1)S(1)}, bf16[2048,256]{1,0:T(8,128)(2,1)}, u32[]{:S(2)}) copy-start(bf16[2048,256]{1,0:T(8,128)(2,1)} %param.12) | copy-start | bytes 3145732
  22.5 19.5 %copy-start.4 = (f32[16,3,256]{2,0,1:T(8,128)S(1)}, f32[16,3,256]{2,0,1:T(8,128)}, u32[]{:S(2)}) copy-start(f32[16,3,256]{2,0,1:T(8,128)} %param.21) | copy-start | bytes 147460
  22.5 19.5 %copy-start.5 = (f32[16,3,256]{2,0,1:T(8,128)S(1)}, f32[16,3,256]{2,0,1:T(8,128)}, u32[]{:S(2)}) copy-start(f32[16,3,256]{2,0,1:T(8,128)} %param.20) | copy-start | bytes 147460
  23.8 37.5 %copy-start = (f32[128,256]{1,0:T(8,128)S(1)}, f32[128,256]{1,0:T(8,128)}, u32[]{:S(2)}) copy-start(f32[128,256]{1,0:T(8,128)} %param.16) | copy-start | bytes 393220
  23.8 48.1 %copy-start.1 = (f32[128,256]{1,0:T(8,128)S(1)}, f32[128,256]{1,0:T(8,128)}, u32[]{:S(2)}) copy-start(f32[128,256]{1,0:T(8,128)} %param.17) | copy-start | bytes 393220
  43.6 41.6 %all-to-all-start.1 = ((f32[16,16,3,256]{3,1,2,0:T(8,128)}), f32[16,16,3,256]{3,1,2,0:T(8,128)S(1)}, u32[]{:S(2)}, u32[]{:S(2)}) async-start(f32[16,16,3,256]{3,1,2,0:T(8,128)} %broadcast_in_dim.4), calls=%async_computation.1 | async-start | bytes 1572864 | tf_op jit(solution)/shard_map/all_to_all | solution.py:33
  47.2 90.0 %all-gather.2.cloned.1.call-start = ((), (), s32[]{:S(2)}) async-start(), calls=%async_computation.2 | async-start | bytes 3342336 | tf_op jit(solution)/shard_map/all_gather | solution.py:47
  85.2 2.7 %copy-start.2 = (f32[256,128]{1,0:T(8,128)S(1)}, f32[256,128]{1,0:T(8,128)}, u32[]{:S(2)}) copy-start(f32[256,128]{1,0:T(8,128)} %param.18) | copy-start | bytes 393220
Sparse Core Ops, SparseCore 0:
  89.5 47.5 all-gather.1
where the time goes:
time: 150 us
  blocking collectives  55.7 us (37%)
  waiting for transfers between devices  44.7 us (30%)
  matrix products  16.1 us (11%)
  between operations  14.3 us (10%)
  local copies, waits for them, and re-layouts  12.2 us (8%)
  starting transfers between devices  3.66 us (2%)
  other arithmetic  2.94 us (2%)
    all_gather x1, waiting for transfers between devices, gather_turned(): lax.all_gather(both, axis, axis=0, tiled=True)  44.7 us
    psum x4, blocking collectives, over_axes(): return functools.reduce(lax.psum, axes, value)  37.7 us
    all_to_all x1, blocking collectives, sum_at_owner(): lax.all_to_all(pieces, axis, split_axis=0, concat_axis=0, tiled=True)  18 us
    unnamed x32, local copies, waits for them, and re-layouts  8.06 us
    dot_general x1, matrix products, on_device(): jnp.dot(normed_input, bases[1], preferred_element_type=jnp.float32)  6.11 us
    all_to_all x1, starting transfers between devices, sent_to_all(): return lax.all_to_all(copies, axis, split_axis=0, concat_axis=0, tiled=True)  3.61 us
    transpose x1, local copies, waits for them, and re-layouts, gather_turned(): finished.append(jnp.moveaxis(piece, 0, dim))  3.11 us
  transfers between devices with their start and end apart: 2, of which 1 were waited for; matrix products, arithmetic and copies ran while one was open for 2% of the time, Pallas kernels for 0%

commit v1 on v0

v1 whole, which is shorter than its diff:
```python
import functools

import jax
import jax.numpy as jnp
from jax import lax
from jax.experimental import pallas as pl
from jax.experimental.pallas import tpu as pltpu
from jax.sharding import Mesh
from jax.sharding import PartitionSpec as P

FS = ("fs_0", "fs_1")
TP = ("tp_0", "tp_1")

NEAR, FAR = 1, 3
STREAMS = (
    (4 * NEAR, 4 * FAR, NEAR, FAR),
    (4 * FAR, 4 * NEAR, FAR, NEAR),
    (NEAR, FAR, 4 * NEAR, 4 * FAR),
    (FAR, NEAR, 4 * FAR, 4 * NEAR),
)
QUARTERS = len(STREAMS)
EARLY = pl.CostEstimate(flops=1 << 34, bytes_accessed=1 << 20, transcendentals=0)
SMALL = pltpu.CompilerParams(vmem_limit_bytes=8 << 20)
LARGE = pltpu.CompilerParams(vmem_limit_bytes=24 << 20)


def fs_of_position(masks, position):
    return functools.reduce(
        lambda a, b: a ^ b, [m for s, m in enumerate(masks) if position >> s & 1], 0
    )


def opening_kernel(out_ref):
    out_ref[...] = jnp.zeros_like(out_ref)


def opening():
    return pl.pallas_call(
        opening_kernel,
        out_shape=jax.ShapeDtypeStruct((8, 128), jnp.float32),
        cost_estimate=EARLY,
        compiler_params=SMALL,
        name="opening",
    )()


def pack_kernel(_, forget_ref, value_ref, out_ref, *packed_refs):
    rows = forget_ref.shape[0] // QUARTERS
    width = out_ref.shape[1]
    tall = out_ref.shape[0] // QUARTERS
    for q, packed in enumerate(packed_refs):
        near = pl.ds(q * rows, rows)
        packed[0, :rows] = forget_ref[near].astype(jnp.bfloat16)
        packed[0, rows : 2 * rows] = value_ref[near].astype(jnp.bfloat16)
        for h in range(tall // rows):
            part = out_ref[pl.ds(q * tall + h * rows, rows)]
            packed[0, 2 * rows :, h * width : (h + 1) * width] = part.astype(jnp.bfloat16)


def pack(opened, *weights):
    rows, columns = weights[0].shape
    shape = jax.ShapeDtypeStruct((1, 3 * rows // QUARTERS, columns), jnp.bfloat16)
    return pl.pallas_call(
        pack_kernel,
        out_shape=(shape,) * QUARTERS,
        cost_estimate=EARLY,
        compiler_params=SMALL,
        name="pack",
    )(opened, *weights)


def reduced_part(x, basis):
    reduced = lax.dot_general(
        basis, x, (((0,), (1,)), ((), ())), preferred_element_type=jnp.float32
    )
    return reduced.astype(jnp.bfloat16)


def projected_part(reduced, cot, factor):
    part = jnp.dot(reduced, cot, preferred_element_type=jnp.float32)
    return (part * factor).astype(jnp.bfloat16)


def moment_kernel(arrived_ref, first_ref, second_ref, one_ref, two_ref, message_ref):
    rows = first_ref.shape[1]
    for k in range(3):
        projected = jnp.sum(arrived_ref[:, k].astype(jnp.float32), axis=0)
        one = 0.9 * first_ref[k] + 0.1 * projected
        two = 0.9 * second_ref[k] + 0.1 * projected * projected
        one_ref[k] = one
        two_ref[k] = two
        direction = (one / (jnp.sqrt(two) + 1e-08)).astype(jnp.bfloat16)
        for i in range(message_ref.shape[0]):
            message_ref[i, k * rows : (k + 1) * rows] = direction


def moments(arrived, first_moment, second_moment):
    _, rows, columns = first_moment.shape
    moment = jax.ShapeDtypeStruct(first_moment.shape, jnp.float32)
    messages = jax.ShapeDtypeStruct((arrived.shape[0], 3 * rows, columns), jnp.bfloat16)
    return pl.pallas_call(
        moment_kernel,
        out_shape=(moment, moment, messages),
        compiler_params=SMALL,
        name="moments",
    )(arrived, first_moment, second_moment)


def square_kernel(arrived_ref, sum_ref):
    rows = arrived_ref.shape[1] // 3
    lane = lax.broadcasted_iota(jnp.int32, sum_ref.shape, 1)
    sums = jnp.zeros(sum_ref.shape, jnp.float32)
    for k in range(3):
        direction = arrived_ref[:, k * rows : (k + 1) * rows].astype(jnp.float32)
        sums = jnp.where(lane == k, jnp.sum(direction * direction), sums)
    sum_ref[...] = sums


def squares(arrived):
    return pl.pallas_call(
        square_kernel,
        out_shape=jax.ShapeDtypeStruct((1, 128), jnp.float32),
        compiler_params=SMALL,
        name="squares",
    )(arrived)


def finish_kernel(entries, me_ref, sums_ref, arrived_ref, base_ref, mine_ref, forget_ref, value_ref, outw_ref, *refs):
    held = [refs[2 * q : 2 * q + 2] for q in range(QUARTERS)]
    (
        new_forget,
        new_value,
        new_out,
        copy_forget,
        copy_value,
        copy_out,
        step_forget,
        step_value,
        step_out,
        dir_ref,
        scale_ref,
    ) = refs[2 * QUARTERS :]
    step = pl.program_id(0)
    owners = arrived_ref.shape[0]
    rank = dir_ref.shape[1]
    rows = rank // owners
    block = mine_ref.shape[1]
    width = outw_ref.shape[1]
    part = block // QUARTERS
    tall = outw_ref.shape[0] // QUARTERS
    me = me_ref[0]
    by_columns = (((1,), (1,)), ((), ()))

    @pl.when(step == 0)
    def _():
        sums = jnp.sum(sums_ref[...], axis=0)
        scale_ref[...] = lax.rsqrt(sums / entries + 1.0)
        for k in range(3):
            direction = arrived_ref[:, k * rows : (k + 1) * rows, :].reshape(rank, -1)
            dir_ref[k] = direction if k < 2 else direction.T
        for k, (old, new, moved) in enumerate(
            ((forget_ref, new_forget, step_forget), (value_ref, new_value, step_value))
        ):
            full = jnp.dot(mine_ref[k], dir_ref[k], preferred_element_type=jnp.float32)
            full = full * scale_ref[0, k]
            moved[...] = full
            new[...] = old[...] - 0.01 * full
        full = lax.dot_general(dir_ref[2], mine_ref[2], by_columns, preferred_element_type=jnp.float32)
        full = full * scale_ref[0, 2]
        step_out[...] = full
        new_out[...] = outw_ref[...] - 0.01 * full

    moves = []
    for k in range(2):
        full = jnp.dot(base_ref[k], dir_ref[k], preferred_element_type=jnp.float32)
        moves.append(full * (0.01 * scale_ref[0, k]))
    full = lax.dot_general(dir_ref[2], base_ref[2], by_columns, preferred_element_type=jnp.float32)
    moves.append(full * (0.01 * scale_ref[0, 2]))
    half = owners // 2
    for j in range(base_ref.shape[1] // block):
        other = me ^ (step * (base_ref.shape[1] // block) + j)
        for q, masks in enumerate(STREAMS):
            position = jnp.int32(0)
            for p in range(owners):
                position = jnp.where(other == fs_of_position(masks, p), p, position)
            early, late = held[q]
            old = jnp.where(position < half, early[position % half], late[position % half])
            old = old.astype(jnp.float32)
            near = slice(j * block + q * part, j * block + (q + 1) * part)
            copy_forget[near] = (old[:part] - moves[0][near]).astype(jnp.bfloat16)
            copy_value[near] = (old[part : 2 * part] - moves[1][near]).astype(jnp.bfloat16)
            for h in range(tall // part):
                down = slice(q * tall + h * part, q * tall + (h + 1) * part)
                across = slice(j * width, (j + 1) * width)
                piece = old[2 * part :, h * width : (h + 1) * width]
                copy_out[down, across] = (piece - moves[2][down, across]).astype(jnp.bfloat16)


def finish(me, sums, arrived, bases, forget_weight, value_weight, out_weight, held, entries, steps=4):
    block, columns = forget_weight.shape
    model, rank = bases.shape[1:]
    tile = model // steps
    whole = lambda a: pl.BlockSpec(a.shape, lambda i, me: (0,) * a.ndim)
    old = (forget_weight, value_weight, out_weight)
    own = [jax.ShapeDtypeStruct(a.shape, jnp.float32) for a in old]
    copies = [jax.ShapeDtypeStruct((model, columns), jnp.bfloat16)] * 2
    copies.append(jax.ShapeDtypeStruct((out_weight.shape[0], model), jnp.bfloat16))
    down = pl.BlockSpec((tile, columns), lambda i, me: (i, 0))
    across = pl.BlockSpec((out_weight.shape[0], tile), lambda i, me: (0, i))
    flat = [a for pair in held for a in pair]
    return pl.pallas_call(
        functools.partial(finish_kernel, entries),
        grid_spec=pltpu.PrefetchScalarGridSpec(
            num_scalar_prefetch=1,
            grid=(steps,),
            in_specs=[
                whole(sums),
                whole(arrived),
                pl.BlockSpec((3, tile, rank), lambda i, me: (0, i, 0)),
                pl.BlockSpec((3, block, rank), lambda i, me: (0, me[0], 0)),
                *map(whole, old),
                *map(whole, flat),
            ],
            out_specs=[
                *map(whole, own),
                down,
                down,
                across,
                *map(whole, own),
            ],
            scratch_shapes=[
                pltpu.VMEM((3, rank, columns), jnp.bfloat16),
                pltpu.VMEM((1, 128), jnp.float32),
            ],
        ),
        out_shape=(*own, *copies, *own),
        compiler_params=LARGE,
        name="finish",
    )(me[None], sums, arrived, bases, bases, *old, *flat)


def swap_all(held, step):
    owners = lax.axis_size(FS)
    received = []
    for masks, value in zip(STREAMS, held):
        pairs = [(i, i ^ masks[step]) for i in range(owners)]
        received.append(lax.ppermute(value, FS, pairs))
    return received


def joined(held, received):
    return [jnp.concatenate(pair) for pair in zip(held, received)]


def on_device(
    normed_input,
    forget_cot,
    value_cot,
    gated_output,
    output_cot,
    forget_weight,
    value_weight,
    out_weight,
    bases,
    first_moment,
    second_moment,
):
    owners = lax.axis_size(FS)
    me = lax.axis_index(FS).astype(jnp.int32)
    factor = float(normed_input.shape[0] * owners) ** (-0.5)
    rank, columns = bases.shape[2], forget_cot.shape[1]
    held = list(pack(opening(), forget_weight, value_weight, out_weight))
    received = swap_all(held, 0)
    inputs = (normed_input, normed_input, output_cot)
    cots = (forget_cot, value_cot, gated_output)
    reduced = [reduced_part(x, bases[k]) for k, x in enumerate(inputs)]
    reduced = lax.optimization_barrier(tuple(reduced))
    parts = [projected_part(r, c, factor) for r, c in zip(reduced, cots)]
    part = jnp.stack([p.reshape(owners, rank // owners, columns) for p in parts], axis=1)
    held = joined(held, received)
    part, *held = lax.optimization_barrier((part, *held))
    arrived = lax.all_to_all(part, FS, split_axis=0, concat_axis=0, tiled=True)
    received = swap_all(held, 1)
    moment_one, moment_two, messages = moments(
        arrived, jnp.moveaxis(first_moment, 1, 0), jnp.moveaxis(second_moment, 1, 0)
    )
    held = joined(held, received)
    messages, *held = lax.optimization_barrier((messages, *held))
    gathered = lax.all_to_all(messages, FS, split_axis=0, concat_axis=0, tiled=True)
    received = swap_all(held, 2)
    sums = squares(gathered)
    held = joined(held, received)
    sums, *held = lax.optimization_barrier((sums, *held))
    received = swap_all(held, 3)
    sums = lax.all_gather(sums, TP, axis=0)
    entries = float(rank * columns * lax.axis_size(TP))
    finished = finish(
        me,
        sums,
        gathered,
        bases,
        forget_weight,
        value_weight,
        out_weight,
        list(zip(held, received)),
        entries,
    )
    moment_one, moment_two = (jnp.moveaxis(m, 0, 1) for m in (moment_one, moment_two))
    return (*finished[:6], moment_one, moment_two, *finished[6:])


def solution(mesh):
    torus = Mesh(mesh.devices.reshape(4, 4, 4, 2), ("fs_0", "fs_1", "tp_0", "tp_1"))
    placed = (
        P(FS, None),
        P(FS, TP),
        P(FS, TP),
        P(FS, TP),
        P(FS, None),
        P(FS, TP),
        P(FS, TP),
        P(TP, FS),
        P(),
        P(FS, None, TP),
        P(FS, None, TP),
    )
    return jax.shard_map(
        on_device,
        mesh=torus,
        in_specs=placed,
        out_specs=(
            P(FS, TP),
            P(FS, TP),
            P(TP, FS),
            P(None, TP),
            P(None, TP),
            P(TP, None),
            P(FS, None, TP),
            P(FS, None, TP),
            P(FS, TP),
            P(FS, TP),
            P(TP, FS),
        ),
        check_vma=False,
    )
```

time: 150 us -> 78.8 us (0.53)
  the two profiles are of different devices: /device:TPU:0 before, /device:TPU:1 now
where the time goes in v1:
time: 78.8 us; the launch traced here: 78.4 us
  starting transfers between devices  30.8 us (39%)
  blocking collectives  14.4 us (18%)
  waiting for transfers between devices  10.9 us (14%)
  matrix products  9.47 us (12%)
  Pallas kernels  5.87 us (7%)
  local copies, waits for them, and re-layouts  4.83 us (6%)
  between operations  1.08 us (1%)
  other arithmetic  1.06 us (1%)
    ppermute x16, starting transfers between devices, swap_all(): received.append(lax.ppermute(value, FS, pairs))  21.1 us
    all_gather x1, blocking collectives, on_device(): sums = lax.all_gather(sums, TP, axis=0)  14.4 us
    ppermute x16, waiting for transfers between devices, swap_all(): received.append(lax.ppermute(value, FS, pairs))  10.9 us
    dot_general x3, matrix products, reduced_part(): lax.dot_general(basis, x, (((0,), (1,)), ((), ())), preferred_element_typ...  8.15 us
    all_to_all x1, starting transfers between devices, on_device(): lax.all_to_all(messages, FS, split_axis=0, concat_axis=0, tiled=True)  5.52 us
    unnamed x34, local copies, waits for them, and re-layouts  4.83 us
    pallas_call x1, Pallas kernels, finish(): pl.pallas_call(functools.partial(finish_kernel, entries), grid_spec=pltpu...  4.76 us
    all_to_all x1, starting transfers between devices, on_device(): arrived = lax.all_to_all(part, FS, split_axis=0, concat_axis=0, tiled=True)  4.13 us
  transfers between devices with their start and end apart: 18, of which 5 were waited for; matrix products, arithmetic and copies ran while one was open for 13% of the time, Pallas kernels for 0%

profile of v1, /device:TPU:1, one launch (start us, length us, event | category | flops | bytes accessed | tf_op | source)
XLA Modules:
  0.0 78.4 jit_solution(5117840866392070172)
XLA Ops:
  0.6 0.0 copy-start
  0.7 0.0 copy-start.6
  0.7 0.0 copy-start.4
  0.7 0.0 slice-start
  0.7 0.9 %copy-done.6 = f32[256,128]{1,0:T(8,128)S(1)} copy-done((f32[256,128]{1,0:T(8,128)S(1)}, f32[256,128]{1,0:T(8,128)}, u32[]{:S(2)}) %copy-start.6) | copy-done | bytes 131096
  1.7 0.1 copy-done.4
  1.7 0.1 copy-done.3
  1.8 2.5 %collective-permute-start = (bf16[1,96,256]{2,1,0:T(8,128)(2,1)S(1)}, bf16[1,96,256]{2,1,0:T(8,128)(2,1)S(1)}, u32[]{:S(2)}, u32[]{:S(2)}) collective-permute-start(bf16[1,96,256]{2,1,0:T(8,128)(2,1)S(1)} %get-tuple-element.48), channel_id=1, source_target_pairs={{0,32},{8,40},{16,48},{24,56},{32,0},{40,8},{48,16},{56,24},{64,96... | collective-permute-start | bytes 147464 | tf_op jit(solution)/shard_map/ppermute | solution.py:247
  4.3 2.2 %collective-permute-start.1 = (bf16[1,96,256]{2,1,0:T(8,128)(2,1)S(1)}, bf16[1,96,256]{2,1,0:T(8,128)(2,1)S(1)}, u32[]{:S(2)}, u32[]{:S(2)}) collective-permute-start(bf16[1,96,256]{2,1,0:T(8,128)(2,1)S(1)} %get-tuple-element.49), channel_id=1, source_target_pairs={{0,96},{8,104},{16,112},{24,120},{32,64},{40,72},{48,80},{56,88},{... | collective-permute-start | bytes 147464 | tf_op jit(solution)/shard_map/ppermute | solution.py:247
  6.6 1.2 %collective-permute-start.2 = (bf16[1,96,256]{2,1,0:T(8,128)(2,1)S(1)}, bf16[1,96,256]{2,1,0:T(8,128)(2,1)S(1)}, u32[]{:S(2)}, u32[]{:S(2)}) collective-permute-start(bf16[1,96,256]{2,1,0:T(8,128)(2,1)S(1)} %get-tuple-element.50), channel_id=1, source_target_pairs={{0,8},{8,0},{16,24},{24,16},{32,40},{40,32},{48,56},{56,48},{64,72... | collective-permute-start | bytes 147464 | tf_op jit(solution)/shard_map/ppermute | solution.py:247
  7.8 1.8 %collective-permute-start.3 = (bf16[1,96,256]{2,1,0:T(8,128)(2,1)S(1)}, bf16[1,96,256]{2,1,0:T(8,128)(2,1)S(1)}, u32[]{:S(2)}, u32[]{:S(2)}) collective-permute-start(bf16[1,96,256]{2,1,0:T(8,128)(2,1)S(1)} %get-tuple-element.51), channel_id=1, source_target_pairs={{0,24},{8,16},{16,8},{24,0},{32,56},{40,48},{48,40},{56,32},{64,88... | collective-permute-start | bytes 147464 | tf_op jit(solution)/shard_map/ppermute | solution.py:247
  9.6 0.0 slice-start.2
  9.6 2.4 %convolution_convert_fusion.1 = bf16[256,2048]{1,0:T(8,128)(2,1)S(1)} fusion(bf16[2048,2048]{1,0:T(8,128)(2,1)S(1)} %bitcast.34, bf16[3,2048,256]{2,1,0:T(8,128)(2,1)S(1)} %copy-done.1), kind=kOutput, calls=%fused_computation.1 | convolution fusion | flops 2148007936 | bytes 10485760 | tf_op jit(solution)/shard_map/dot_general | solution.py:73
  12.0 0.0 slice-start.3
  12.1 3.4 %convolution_convert_fusion.2 = bf16[256,2048]{1,0:T(8,128)(2,1)} fusion(bf16[2048,2048]{1,0:T(8,128)(2,1)S(1)} %bitcast.34, bf16[3,2048,256]{2,1,0:T(8,128)(2,1)S(1)} %copy-done.1), kind=kOutput, calls=%fused_computation.2 | convolution fusion | flops 2148007936 | bytes 10485760 | tf_op jit(solution)/shard_map/dot_general | solution.py:73
  15.4 0.0 copy-start.10
  15.4 0.0 copy-start.11
  15.5 2.4 %convolution_convert_fusion = bf16[256,2048]{1,0:T(8,128)(2,1)S(1)} fusion(bf16[2048,2048]{1,0:T(8,128)(2,1)S(1)} %bitcast.36, bf16[3,2048,256]{2,1,0:T(8,128)(2,1)S(1)} %copy-done.1), kind=kOutput, calls=%fused_computation | convolution fusion | flops 2148007936 | bytes 10485760 | tf_op jit(solution)/shard_map/dot_general | solution.py:73
  17.9 0.0 copy-start.9
  17.9 0.4 fusion
  18.4 0.4 fusion.1
  18.8 0.4 fusion.2
  19.3 0.8 %pad_maximum_fusion = bf16[16,3,16,256]{3,2,1,0:T(8,128)(2,1)} fusion(bf16[16,1,16,256]{3,2,1,0:T(8,128)(2,1)S(1)} %bitcast.32, bf16[16,1,16,256]{3,2,1,0:T(8,128)(2,1)S(1)} %bitcast.31, bf16[16,1,16,256]{3,2,1,0:T(8,128)(2,1)S(1)} %bitcast.30), kind=kLoop, calls=%fused_computation.15 | loop fusion | flops 393216 | bytes 786432 | tf_op jit(solution)/shard_map/stack | solution.py:279
  20.2 0.6 collective-permute-start.4
  20.8 4.1 %all-to-all-start = ((bf16[16,3,16,256]{3,2,1,0:T(8,128)(2,1)}), bf16[16,3,16,256]{3,2,1,0:T(8,128)(2,1)S(1)}, u32[]{:S(2)}, u32[]{:S(2)}) async-start(bf16[16,3,16,256]{3,2,1,0:T(8,128)(2,1)} %pad_maximum_fusion), calls=%async_computation | async-start | bytes 786432 | tf_op jit(solution)/shard_map/all_to_all | solution.py:282
  24.9 1.4 %collective-permute-start.5 = (bf16[2,96,256]{2,1,0:T(8,128)(2,1)S(1)}, bf16[2,96,256]{2,1,0:T(8,128)(2,1)S(1)}, u32[]{:S(2)}, u32[]{:S(2)}) collective-permute-start(bf16[2,96,256]{2,1,0:T(8,128)(2,1)S(1)} %pad_maximum_fusion.10), channel_id=1, source_target_pairs={{0,32},{8,40},{16,48},{24,56},{32,0},{40,8},{48,16},{56,24},{64,96... | collective-permute-start | bytes 294920 | tf_op jit(solution)/shard_map/ppermute | solution.py:247
  26.3 2.4 %collective-permute-start.6 = (bf16[2,96,256]{2,1,0:T(8,128)(2,1)S(1)}, bf16[2,96,256]{2,1,0:T(8,128)(2,1)S(1)}, u32[]{:S(2)}, u32[]{:S(2)}) collective-permute-start(bf16[2,96,256]{2,1,0:T(8,128)(2,1)S(1)} %pad_maximum_fusion.11), channel_id=1, source_target_pairs={{0,24},{8,16},{16,8},{24,0},{32,56},{40,48},{48,40},{56,32},{64,88... | collective-permute-start | bytes 294920 | tf_op jit(solution)/shard_map/ppermute | solution.py:247
  28.7 0.4 collective-permute-done.5
  29.1 4.1 %collective-permute-done.6 = bf16[2,96,256]{2,1,0:T(8,128)(2,1)S(1)} collective-permute-done((bf16[2,96,256]{2,1,0:T(8,128)(2,1)S(1)}, bf16[2,96,256]{2,1,0:T(8,128)(2,1)S(1)}, u32[]{:S(2)}, u32[]{:S(2)}) %collective-permute-start.6) | collective-permute-done | bytes 98336 | tf_op jit(solution)/shard_map/ppermute | solution.py:247
  33.3 0.2 collective-permute-done.7
  33.5 0.9 %moments.1 = (f32[3,16,256]{2,1,0:T(8,128)}, f32[3,16,256]{2,1,0:T(8,128)}, bf16[16,48,256]{2,1,0:T(8,128)(2,1)}) custom-call(bf16[16,3,16,256]{3,2,1,0:T(8,128)(2,1)S(1)} %all-to-all-done.arrived_ref, f32[3,16,256]{2,1,0:T(8,128)S(1)} %bitcast.27, f32[3,16,256]{2,1,0:T(8,128)S(1)} %bitcast.28), custom_call_target="tpu_custom_call" | custom-call | tf_op jit(solution)/shard_map/moments/pallas_call | solution.py:101
  34.4 0.0 collective-permute-start.8
  34.4 1.3 %collective-permute-start.9 = (bf16[4,96,256]{2,1,0:T(8,128)(2,1)S(1)}, bf16[4,96,256]{2,1,0:T(8,128)(2,1)S(1)}, u32[]{:S(2)}, u32[]{:S(2)}) collective-permute-start(bf16[4,96,256]{2,1,0:T(8,128)(2,1)S(1)} %pad_maximum_fusion.6), channel_id=1, source_target_pairs={{0,24},{8,16},{16,8},{24,0},{32,56},{40,48},{48,40},{56,32},{64,88... | collective-permute-start | bytes 589832 | tf_op jit(solution)/shard_map/ppermute | solution.py:247
  35.7 5.5 %all-to-all-start.1 = ((bf16[16,48,256]{2,1,0:T(8,128)(2,1)}), bf16[16,48,256]{2,1,0:T(8,128)(2,1)S(1)}, u32[]{:S(2)}, u32[]{:S(2)}) async-start(bf16[16,48,256]{2,1,0:T(8,128)(2,1)} %get-tuple-element.58), calls=%async_computation.1 | async-start | bytes 786432 | tf_op jit(solution)/shard_map/all_to_all | solution.py:289
  41.2 1.4 %collective-permute-start.10 = (bf16[4,96,256]{2,1,0:T(8,128)(2,1)S(1)}, bf16[4,96,256]{2,1,0:T(8,128)(2,1)S(1)}, u32[]{:S(2)}, u32[]{:S(2)}) collective-permute-start(bf16[4,96,256]{2,1,0:T(8,128)(2,1)S(1)} %pad_maximum_fusion.7), channel_id=1, source_target_pairs={{0,32},{8,40},{16,48},{24,56},{32,0},{40,8},{48,16},{56,24},{64,96... | collective-permute-start | bytes 589832 | tf_op jit(solution)/shard_map/ppermute | solution.py:247
  42.6 1.9 %collective-permute-start.11 = (bf16[4,96,256]{2,1,0:T(8,128)(2,1)S(1)}, bf16[4,96,256]{2,1,0:T(8,128)(2,1)S(1)}, u32[]{:S(2)}, u32[]{:S(2)}) collective-permute-start(bf16[4,96,256]{2,1,0:T(8,128)(2,1)S(1)} %pad_maximum_fusion.8), channel_id=1, source_target_pairs={{0,96},{8,104},{16,112},{24,120},{32,64},{40,72},{48,80},{56,88},{... | collective-permute-start | bytes 589832 | tf_op jit(solution)/shard_map/ppermute | solution.py:247
  44.6 3.4 %collective-permute-done.10 = bf16[4,96,256]{2,1,0:T(8,128)(2,1)S(1)} collective-permute-done((bf16[4,96,256]{2,1,0:T(8,128)(2,1)S(1)}, bf16[4,96,256]{2,1,0:T(8,128)(2,1)S(1)}, u32[]{:S(2)}, u32[]{:S(2)}) %collective-permute-start.10) | collective-permute-done | bytes 196640 | tf_op jit(solution)/shard_map/ppermute | solution.py:247
  48.0 2.7 %collective-permute-done.11 = bf16[4,96,256]{2,1,0:T(8,128)(2,1)S(1)} collective-permute-done((bf16[4,96,256]{2,1,0:T(8,128)(2,1)S(1)}, bf16[4,96,256]{2,1,0:T(8,128)(2,1)S(1)}, u32[]{:S(2)}, u32[]{:S(2)}) %collective-permute-start.11) | collective-permute-done | bytes 196640 | tf_op jit(solution)/shard_map/ppermute | solution.py:247
  50.8 0.2 squares.1
  51.0 2.1 %collective-permute-start.12 = (bf16[8,96,256]{2,1,0:T(8,128)(2,1)S(1)}, bf16[8,96,256]{2,1,0:T(8,128)(2,1)S(1)}, u32[]{:S(2)}, u32[]{:S(2)}) collective-permute-start(bf16[8,96,256]{2,1,0:T(8,128)(2,1)S(1)} %pad_maximum_fusion.1.refs_0_), channel_id=1, source_target_pairs={{0,24},{8,16},{16,8},{24,0},{32,56},{40,48},{48,40},{56,32},{64,88... | collective-permute-start | bytes 1179656 | tf_op jit(solution)/shard_map/ppermute | solution.py:247
  53.1 1.2 %collective-permute-start.13 = (bf16[8,96,256]{2,1,0:T(8,128)(2,1)S(1)}, bf16[8,96,256]{2,1,0:T(8,128)(2,1)}, u32[]{:S(2)}, u32[]{:S(2)}) collective-permute-start(bf16[8,96,256]{2,1,0:T(8,128)(2,1)S(1)} %pad_maximum_fusion.2.refs_2_), channel_id=1, source_target_pairs={{0,8},{8,0},{16,24},{24,16},{32,40},{40,32},{48,56},{56,48},{64,72... | collective-permute-start | bytes 1179656 | tf_op jit(solution)/shard_map/ppermute | solution.py:247
  54.3 1.1 %collective-permute-start.14 = (bf16[8,96,256]{2,1,0:T(8,128)(2,1)S(1)}, bf16[8,96,256]{2,1,0:T(8,128)(2,1)}, u32[]{:S(2)}, u32[]{:S(2)}) collective-permute-start(bf16[8,96,256]{2,1,0:T(8,128)(2,1)S(1)} %pad_maximum_fusion.3.refs_4_), channel_id=1, source_target_pairs={{0,96},{8,104},{16,112},{24,120},{32,64},{40,72},{48,80},{56,88},{... | collective-permute-start | bytes 1179656 | tf_op jit(solution)/shard_map/ppermute | solution.py:247
  55.4 14.4 %all-gather.1.sums_ref = f32[8,1,128]{2,1,0:T(1,128)S(1)} all-gather(f32[1,1,128]{2,1,0:T(1,128)S(1)} %bitcast.29), channel_id=2, replica_groups=mesh['fs_0'=4,'fs_1'=4,'tp_0'=4,'tp_1'=2] {'tp_0','tp_1'}, dimensions={0}, use_global_device_ids=true | all-gather | bytes 4608 | tf_op jit(solution)/shard_map/all_gather | solution.py:295
  69.8 0.0 copy-start.2
  69.9 1.9 %copy-done.2 = bf16[3,2048,256]{2,1,0:T(8,128)(2,1)S(1)} copy-done((bf16[3,2048,256]{2,1,0:T(8,128)(2,1)S(1)}, bf16[3,2048,256]{2,1,0:T(8,128)(2,1)}, u32[]{:S(2)}) %copy-start.2) | copy-done | bytes 3145752
  71.7 0.9 %copy-done.5 = f32[128,256]{1,0:T(8,128)S(1)} copy-done((f32[128,256]{1,0:T(8,128)S(1)}, f32[128,256]{1,0:T(8,128)}, u32[]{:S(2)}) %copy-start.5) | copy-done | bytes 131096
  72.6 0.9 %copy-done.7 = f32[256,128]{1,0:T(8,128)S(1)} copy-done((f32[256,128]{1,0:T(8,128)S(1)}, f32[256,128]{1,0:T(8,128)}, u32[]{:S(2)}) %copy-start.7) | copy-done | bytes 131096
  73.5 4.8 %finish.1 = (f32[128,256]{1,0:T(8,128)}, f32[128,256]{1,0:T(8,128)}, f32[256,128]{1,0:T(8,128)}, bf16[2048,256]{1,0:T(8,128)(2,1)}, bf16[2048,256]{1,0:T(8,128)(...) custom-call(s32[1]{0:T(128)} %bitcast.me_ref, ...), custom_call_target="tpu_custom_call" | custom-call | tf_op jit(solution)/shard_map/finish/pallas_call | solution.py:211
  (49 shorter events, 0.4 us)
Async XLA Ops:
  0.6 17.2 %copy-start = (bf16[2048,256]{1,0:T(8,128)(2,1)S(1)}, bf16[2048,256]{1,0:T(8,128)(2,1)}, u32[]{:S(2)}) copy-start(bf16[2048,256]{1,0:T(8,128)(2,1)} %param.12) | copy-start | bytes 3145732
  0.7 1.0 %copy-start.6 = (f32[256,128]{1,0:T(8,128)S(1)}, f32[256,128]{1,0:T(8,128)}, u32[]{:S(2)}) copy-start(f32[256,128]{1,0:T(8,128)} %outw_ref.1) | copy-start | bytes 393220
  0.7 1.0 %copy-start.4 = (f32[128,256]{1,0:T(8,128)S(1)}, f32[128,256]{1,0:T(8,128)}, u32[]{:S(2)}) copy-start(f32[128,256]{1,0:T(8,128)} %value_ref.3) | copy-start | bytes 393220
  0.7 1.1 %copy-start.3 = (f32[128,256]{1,0:T(8,128)S(1)}, f32[128,256]{1,0:T(8,128)}, u32[]{:S(2)}) copy-start(f32[128,256]{1,0:T(8,128)} %forget_ref.3) | copy-start | bytes 393220
  0.7 8.9 %slice-start = ((s8[8388608]{0:T(1024)(128)(4,1)}), s8[4194304]{0:T(1024)(128)(4,1)S(1)}, s32[]{:S(2)}) async-start(s8[8388608]{0:T(1024)(128)(4,1)} %bitcast.33), calls=%async_computation.2 | async-start | bytes 8388608
  1.8 7.8 %copy-start.1 = (bf16[3,2048,256]{2,1,0:T(8,128)(2,1)S(1)}, bf16[3,2048,256]{2,1,0:T(8,128)(2,1)}, u32[]{:S(2)}) copy-start(bf16[3,2048,256]{2,1,0:T(8,128)(2,1)} %mine_ref.1) | copy-start | bytes 9437188
  1.8 7.8 %slice-start.1 = ((s8[8388608]{0:T(1024)(128)(4,1)}), s8[4194304]{0:T(1024)(128)(4,1)S(1)}, s32[]{:S(2)}) async-start(s8[8388608]{0:T(1024)(128)(4,1)} %bitcast.33), calls=%async_computation.3 | async-start | bytes 8388608
  1.8 18.2 %collective-permute-start = (bf16[1,96,256]{2,1,0:T(8,128)(2,1)S(1)}, bf16[1,96,256]{2,1,0:T(8,128)(2,1)S(1)}, u32[]{:S(2)}, u32[]{:S(2)}) collective-permute-start(bf16[1,96,256]{2,1,0:T(8,128)(2,1)S(1)} %get-tuple-element.48), channel_id=1, source_target_pairs={{0,32},{8,40},{16,48},{24,56},{32,0},{40,8},{48,16},{56,24},{64,96... | collective-permute-start | bytes 147464 | tf_op jit(solution)/shard_map/ppermute | solution.py:247
  4.3 15.7 %collective-permute-start.1 = (bf16[1,96,256]{2,1,0:T(8,128)(2,1)S(1)}, bf16[1,96,256]{2,1,0:T(8,128)(2,1)S(1)}, u32[]{:S(2)}, u32[]{:S(2)}) collective-permute-start(bf16[1,96,256]{2,1,0:T(8,128)(2,1)S(1)} %get-tuple-element.49), channel_id=1, source_target_pairs={{0,96},{8,104},{16,112},{24,120},{32,64},{40,72},{48,80},{56,88},{... | collective-permute-start | bytes 147464 | tf_op jit(solution)/shard_map/ppermute | solution.py:247
  6.6 13.5 %collective-permute-start.2 = (bf16[1,96,256]{2,1,0:T(8,128)(2,1)S(1)}, bf16[1,96,256]{2,1,0:T(8,128)(2,1)S(1)}, u32[]{:S(2)}, u32[]{:S(2)}) collective-permute-start(bf16[1,96,256]{2,1,0:T(8,128)(2,1)S(1)} %get-tuple-element.50), channel_id=1, source_target_pairs={{0,8},{8,0},{16,24},{24,16},{32,40},{40,32},{48,56},{56,48},{64,72... | collective-permute-start | bytes 147464 | tf_op jit(solution)/shard_map/ppermute | solution.py:247
  7.8 12.3 %collective-permute-start.3 = (bf16[1,96,256]{2,1,0:T(8,128)(2,1)S(1)}, bf16[1,96,256]{2,1,0:T(8,128)(2,1)S(1)}, u32[]{:S(2)}, u32[]{:S(2)}) collective-permute-start(bf16[1,96,256]{2,1,0:T(8,128)(2,1)S(1)} %get-tuple-element.51), channel_id=1, source_target_pairs={{0,24},{8,16},{16,8},{24,0},{32,56},{40,48},{48,40},{56,32},{64,88... | collective-permute-start | bytes 147464 | tf_op jit(solution)/shard_map/ppermute | solution.py:247
  9.6 5.8 %slice-start.2 = ((s8[8388608]{0:T(1024)(128)(4,1)}), s8[4194304]{0:T(1024)(128)(4,1)S(1)}, s32[]{:S(2)}) async-start(s8[8388608]{0:T(1024)(128)(4,1)} %bitcast.35), calls=%async_computation.4 | async-start | bytes 8388608
  12.0 3.4 %slice-start.3 = ((s8[8388608]{0:T(1024)(128)(4,1)}), s8[4194304]{0:T(1024)(128)(4,1)S(1)}, s32[]{:S(2)}) async-start(s8[8388608]{0:T(1024)(128)(4,1)} %bitcast.35), calls=%async_computation.5 | async-start | bytes 8388608
  15.4 2.4 %copy-start.12 = (bf16[256,2048]{1,0:T(8,128)(2,1)S(1)}, bf16[256,2048]{1,0:T(8,128)(2,1)}, u32[]{:S(2)}) copy-start(bf16[256,2048]{1,0:T(8,128)(2,1)} %convolution_convert_fusion.2) | copy-start | bytes 3145732
  15.4 2.9 %copy-start.10 = (bf16[2048,256]{1,0:T(8,128)(2,1)S(1)}, bf16[2048,256]{1,0:T(8,128)(2,1)}, u32[]{:S(2)}) copy-start(bf16[2048,256]{1,0:T(8,128)(2,1)} %param.13) | copy-start | bytes 3145732
  15.4 3.4 %copy-start.11 = (bf16[2048,256]{1,0:T(8,128)(2,1)S(1)}, bf16[2048,256]{1,0:T(8,128)(2,1)}, u32[]{:S(2)}) copy-start(bf16[2048,256]{1,0:T(8,128)(2,1)} %param.14) | copy-start | bytes 3145732
  17.9 15.6 %copy-start.8 = (f32[16,3,256]{2,0,1:T(8,128)S(1)}, f32[16,3,256]{2,0,1:T(8,128)}, u32[]{:S(2)}) copy-start(f32[16,3,256]{2,0,1:T(8,128)} %param.20) | copy-start | bytes 147460
  17.9 15.6 %copy-start.9 = (f32[16,3,256]{2,0,1:T(8,128)S(1)}, f32[16,3,256]{2,0,1:T(8,128)}, u32[]{:S(2)}) copy-start(f32[16,3,256]{2,0,1:T(8,128)} %param.21) | copy-start | bytes 147460
  20.2 8.5 %collective-permute-start.4 = (bf16[2,96,256]{2,1,0:T(8,128)(2,1)S(1)}, bf16[2,96,256]{2,1,0:T(8,128)(2,1)S(1)}, u32[]{:S(2)}, u32[]{:S(2)}) collective-permute-start(bf16[2,96,256]{2,1,0:T(8,128)(2,1)S(1)} %pad_maximum_fusion.9), channel_id=1, source_target_pairs={{0,96},{8,104},{16,112},{24,120},{32,64},{40,72},{48,80},{56,88},{... | collective-permute-start | bytes 294920 | tf_op jit(solution)/shard_map/ppermute | solution.py:247
  20.8 12.7 %all-to-all-start = ((bf16[16,3,16,256]{3,2,1,0:T(8,128)(2,1)}), bf16[16,3,16,256]{3,2,1,0:T(8,128)(2,1)S(1)}, u32[]{:S(2)}, u32[]{:S(2)}) async-start(bf16[16,3,16,256]{3,2,1,0:T(8,128)(2,1)} %pad_maximum_fusion), calls=%async_computation | async-start | bytes 786432 | tf_op jit(solution)/shard_map/all_to_all | solution.py:282
  24.9 4.2 %collective-permute-start.5 = (bf16[2,96,256]{2,1,0:T(8,128)(2,1)S(1)}, bf16[2,96,256]{2,1,0:T(8,128)(2,1)S(1)}, u32[]{:S(2)}, u32[]{:S(2)}) collective-permute-start(bf16[2,96,256]{2,1,0:T(8,128)(2,1)S(1)} %pad_maximum_fusion.10), channel_id=1, source_target_pairs={{0,32},{8,40},{16,48},{24,56},{32,0},{40,8},{48,16},{56,24},{64,96... | collective-permute-start | bytes 294920 | tf_op jit(solution)/shard_map/ppermute | solution.py:247
  26.3 7.0 %collective-permute-start.6 = (bf16[2,96,256]{2,1,0:T(8,128)(2,1)S(1)}, bf16[2,96,256]{2,1,0:T(8,128)(2,1)S(1)}, u32[]{:S(2)}, u32[]{:S(2)}) collective-permute-start(bf16[2,96,256]{2,1,0:T(8,128)(2,1)S(1)} %pad_maximum_fusion.11), channel_id=1, source_target_pairs={{0,24},{8,16},{16,8},{24,0},{32,56},{40,48},{48,40},{56,32},{64,88... | collective-permute-start | bytes 294920 | tf_op jit(solution)/shard_map/ppermute | solution.py:247
  28.7 4.8 %collective-permute-start.7 = (bf16[2,96,256]{2,1,0:T(8,128)(2,1)S(1)}, bf16[2,96,256]{2,1,0:T(8,128)(2,1)S(1)}, u32[]{:S(2)}, u32[]{:S(2)}) collective-permute-start(bf16[2,96,256]{2,1,0:T(8,128)(2,1)S(1)} %pad_maximum_fusion.12), channel_id=1, source_target_pairs={{0,8},{8,0},{16,24},{24,16},{32,40},{40,32},{48,56},{56,48},{64,72... | collective-permute-start | bytes 294920 | tf_op jit(solution)/shard_map/ppermute | solution.py:247
  34.4 10.1 %collective-permute-start.8 = (bf16[4,96,256]{2,1,0:T(8,128)(2,1)S(1)}, bf16[4,96,256]{2,1,0:T(8,128)(2,1)S(1)}, u32[]{:S(2)}, u32[]{:S(2)}) collective-permute-start(bf16[4,96,256]{2,1,0:T(8,128)(2,1)S(1)} %pad_maximum_fusion.5), channel_id=1, source_target_pairs={{0,8},{8,0},{16,24},{24,16},{32,40},{40,32},{48,56},{56,48},{64,72... | collective-permute-start | bytes 589832 | tf_op jit(solution)/shard_map/ppermute | solution.py:247
  34.4 10.1 %collective-permute-start.9 = (bf16[4,96,256]{2,1,0:T(8,128)(2,1)S(1)}, bf16[4,96,256]{2,1,0:T(8,128)(2,1)S(1)}, u32[]{:S(2)}, u32[]{:S(2)}) collective-permute-start(bf16[4,96,256]{2,1,0:T(8,128)(2,1)S(1)} %pad_maximum_fusion.6), channel_id=1, source_target_pairs={{0,24},{8,16},{16,8},{24,0},{32,56},{40,48},{48,40},{56,32},{64,88... | collective-permute-start | bytes 589832 | tf_op jit(solution)/shard_map/ppermute | solution.py:247
  35.7 15.1 %all-to-all-start.1 = ((bf16[16,48,256]{2,1,0:T(8,128)(2,1)}), bf16[16,48,256]{2,1,0:T(8,128)(2,1)S(1)}, u32[]{:S(2)}, u32[]{:S(2)}) async-start(bf16[16,48,256]{2,1,0:T(8,128)(2,1)} %get-tuple-element.58), calls=%async_computation.1 | async-start | bytes 786432 | tf_op jit(solution)/shard_map/all_to_all | solution.py:289
  41.2 6.8 %collective-permute-start.10 = (bf16[4,96,256]{2,1,0:T(8,128)(2,1)S(1)}, bf16[4,96,256]{2,1,0:T(8,128)(2,1)S(1)}, u32[]{:S(2)}, u32[]{:S(2)}) collective-permute-start(bf16[4,96,256]{2,1,0:T(8,128)(2,1)S(1)} %pad_maximum_fusion.7), channel_id=1, source_target_pairs={{0,32},{8,40},{16,48},{24,56},{32,0},{40,8},{48,16},{56,24},{64,96... | collective-permute-start | bytes 589832 | tf_op jit(solution)/shard_map/ppermute | solution.py:247
  42.6 8.1 %collective-permute-start.11 = (bf16[4,96,256]{2,1,0:T(8,128)(2,1)S(1)}, bf16[4,96,256]{2,1,0:T(8,128)(2,1)S(1)}, u32[]{:S(2)}, u32[]{:S(2)}) collective-permute-start(bf16[4,96,256]{2,1,0:T(8,128)(2,1)S(1)} %pad_maximum_fusion.8), channel_id=1, source_target_pairs={{0,96},{8,104},{16,112},{24,120},{32,64},{40,72},{48,80},{56,88},{... | collective-permute-start | bytes 589832 | tf_op jit(solution)/shard_map/ppermute | solution.py:247
  51.0 18.8 %collective-permute-start.12 = (bf16[8,96,256]{2,1,0:T(8,128)(2,1)S(1)}, bf16[8,96,256]{2,1,0:T(8,128)(2,1)S(1)}, u32[]{:S(2)}, u32[]{:S(2)}) collective-permute-start(bf16[8,96,256]{2,1,0:T(8,128)(2,1)S(1)} %pad_maximum_fusion.1.refs_0_), channel_id=1, source_target_pairs={{0,24},{8,16},{16,8},{24,0},{32,56},{40,48},{48,40},{56,32},{64,88... | collective-permute-start | bytes 1179656 | tf_op jit(solution)/shard_map/ppermute | solution.py:247
  53.1 16.7 %collective-permute-start.13 = (bf16[8,96,256]{2,1,0:T(8,128)(2,1)S(1)}, bf16[8,96,256]{2,1,0:T(8,128)(2,1)}, u32[]{:S(2)}, u32[]{:S(2)}) collective-permute-start(bf16[8,96,256]{2,1,0:T(8,128)(2,1)S(1)} %pad_maximum_fusion.2.refs_2_), channel_id=1, source_target_pairs={{0,8},{8,0},{16,24},{24,16},{32,40},{40,32},{48,56},{56,48},{64,72... | collective-permute-start | bytes 1179656 | tf_op jit(solution)/shard_map/ppermute | solution.py:247
  54.3 15.5 %collective-permute-start.14 = (bf16[8,96,256]{2,1,0:T(8,128)(2,1)S(1)}, bf16[8,96,256]{2,1,0:T(8,128)(2,1)}, u32[]{:S(2)}, u32[]{:S(2)}) collective-permute-start(bf16[8,96,256]{2,1,0:T(8,128)(2,1)S(1)} %pad_maximum_fusion.3.refs_4_), channel_id=1, source_target_pairs={{0,96},{8,104},{16,112},{24,120},{32,64},{40,72},{48,80},{56,88},{... | collective-permute-start | bytes 1179656 | tf_op jit(solution)/shard_map/ppermute | solution.py:247
  55.4 14.4 %collective-permute-start.15 = (bf16[8,96,256]{2,1,0:T(8,128)(2,1)S(1)}, bf16[8,96,256]{2,1,0:T(8,128)(2,1)}, u32[]{:S(2)}, u32[]{:S(2)}) collective-permute-start(bf16[8,96,256]{2,1,0:T(8,128)(2,1)S(1)} %pad_maximum_fusion.4.refs_6_), channel_id=1, source_target_pairs={{0,32},{8,40},{16,48},{24,56},{32,0},{40,8},{48,16},{56,24},{64,96... | collective-permute-start | bytes 1179656 | tf_op jit(solution)/shard_map/ppermute | solution.py:247
  69.8 1.9 %copy-start.2 = (bf16[3,2048,256]{2,1,0:T(8,128)(2,1)S(1)}, bf16[3,2048,256]{2,1,0:T(8,128)(2,1)}, u32[]{:S(2)}) copy-start(bf16[3,2048,256]{2,1,0:T(8,128)(2,1)} %mine_ref.1) | copy-start | bytes 9437188
  71.7 0.9 %copy-start.5 = (f32[128,256]{1,0:T(8,128)S(1)}, f32[128,256]{1,0:T(8,128)}, u32[]{:S(2)}) copy-start(f32[128,256]{1,0:T(8,128)} %value_ref.3) | copy-start | bytes 393220
  72.6 0.9 %copy-start.7 = (f32[256,128]{1,0:T(8,128)S(1)}, f32[256,128]{1,0:T(8,128)}, u32[]{:S(2)}) copy-start(f32[256,128]{1,0:T(8,128)} %outw_ref.1) | copy-start | bytes 393220

commit v2 on v1

--- a/solution.py
+++ b/solution.py
@@ -8,26 +8,16 @@
 from jax.sharding import Mesh
 from jax.sharding import PartitionSpec as P
 
+
 FS = ("fs_0", "fs_1")
 TP = ("tp_0", "tp_1")
 
 NEAR, FAR = 1, 3
-STREAMS = (
-    (4 * NEAR, 4 * FAR, NEAR, FAR),
-    (4 * FAR, 4 * NEAR, FAR, NEAR),
-    (NEAR, FAR, 4 * NEAR, 4 * FAR),
-    (FAR, NEAR, 4 * FAR, 4 * NEAR),
-)
-QUARTERS = len(STREAMS)
+SIDE = 4
+TURNS = ((NEAR, FAR), (FAR, NEAR))
 EARLY = pl.CostEstimate(flops=1 << 34, bytes_accessed=1 << 20, transcendentals=0)
 SMALL = pltpu.CompilerParams(vmem_limit_bytes=8 << 20)
 LARGE = pltpu.CompilerParams(vmem_limit_bytes=24 << 20)
-
-
-def fs_of_position(masks, position):
-    return functools.reduce(
-        lambda a, b: a ^ b, [m for s, m in enumerate(masks) if position >> s & 1], 0
-    )
 
 
 def opening_kernel(out_ref):
@@ -44,25 +34,21 @@
     )()
 
 
-def pack_kernel(_, forget_ref, value_ref, out_ref, *packed_refs):
-    rows = forget_ref.shape[0] // QUARTERS
+def pack_kernel(_, forget_ref, value_ref, out_ref, packed_ref):
+    rows = forget_ref.shape[0]
     width = out_ref.shape[1]
-    tall = out_ref.shape[0] // QUARTERS
-    for q, packed in enumerate(packed_refs):
-        near = pl.ds(q * rows, rows)
-        packed[0, :rows] = forget_ref[near].astype(jnp.bfloat16)
-        packed[0, rows : 2 * rows] = value_ref[near].astype(jnp.bfloat16)
-        for h in range(tall // rows):
-            part = out_ref[pl.ds(q * tall + h * rows, rows)]
-            packed[0, 2 * rows :, h * width : (h + 1) * width] = part.astype(jnp.bfloat16)
+    packed_ref[0, :rows] = forget_ref[...].astype(jnp.bfloat16)
+    packed_ref[0, rows : 2 * rows] = value_ref[...].astype(jnp.bfloat16)
+    for h in range(out_ref.shape[0] // rows):
+        part = out_ref[pl.ds(h * rows, rows)]
+        packed_ref[0, 2 * rows :, h * width : (h + 1) * width] = part.astype(jnp.bfloat16)
 
 
 def pack(opened, *weights):
     rows, columns = weights[0].shape
-    shape = jax.ShapeDtypeStruct((1, 3 * rows // QUARTERS, columns), jnp.bfloat16)
     return pl.pallas_call(
         pack_kernel,
-        out_shape=(shape,) * QUARTERS,
+        out_shape=jax.ShapeDtypeStruct((1, 3 * rows, columns), jnp.bfloat16),
         cost_estimate=EARLY,
         compiler_params=SMALL,
         name="pack",
@@ -97,7 +83,7 @@
 def moments(arrived, first_moment, second_moment):
     _, rows, columns = first_moment.shape
     moment = jax.ShapeDtypeStruct(first_moment.shape, jnp.float32)
-    messages = jax.ShapeDtypeStruct((arrived.shape[0], 3 * rows, columns), jnp.bfloat16)
+    messages = pltpu.HBM((arrived.shape[0], 3 * rows, columns), jnp.bfloat16)
     return pl.pallas_call(
         moment_kernel,
         out_shape=(moment, moment, messages),
@@ -108,7 +94,7 @@
 
 def square_kernel(arrived_ref, sum_ref):
     rows = arrived_ref.shape[1] // 3
-    lane = lax.broadcasted_iota(jnp.int32, sum_ref.shape, 1)
+    lane = lax.broadcasted_iota(jnp.int32, sum_ref.shape, 2)
     sums = jnp.zeros(sum_ref.shape, jnp.float32)
     for k in range(3):
         direction = arrived_ref[:, k * rows : (k + 1) * rows].astype(jnp.float32)
@@ -116,17 +102,21 @@
     sum_ref[...] = sums
 
 
-def squares(arrived):
+def squares(arrived, copies):
     return pl.pallas_call(
         square_kernel,
-        out_shape=jax.ShapeDtypeStruct((1, 128), jnp.float32),
+        out_shape=jax.ShapeDtypeStruct((copies, 1, 128), jnp.float32),
         compiler_params=SMALL,
         name="squares",
     )(arrived)
 
 
 def finish_kernel(entries, me_ref, sums_ref, arrived_ref, base_ref, mine_ref, forget_ref, value_ref, outw_ref, *refs):
-    held = [refs[2 * q : 2 * q + 2] for q in range(QUARTERS)]
+    streams = len(TURNS)
+    held = []
+    for t in range(streams):
+        whole, nearer, even, odd, across = refs[5 * t : 5 * t + 5]
+        held.append((whole, nearer, (even, odd), across))
     (
         new_forget,
         new_value,
@@ -139,15 +129,14 @@
         step_out,
         dir_ref,
         scale_ref,
-    ) = refs[2 * QUARTERS :]
+        old_ref,
+    ) = refs[5 * streams :]
     step = pl.program_id(0)
     owners = arrived_ref.shape[0]
     rank = dir_ref.shape[1]
     rows = rank // owners
     block = mine_ref.shape[1]
     width = outw_ref.shape[1]
-    part = block // QUARTERS
-    tall = outw_ref.shape[0] // QUARTERS
     me = me_ref[0]
     by_columns = (((1,), (1,)), ((), ()))
 
@@ -176,24 +165,33 @@
         moves.append(full * (0.01 * scale_ref[0, k]))
     full = lax.dot_general(dir_ref[2], base_ref[2], by_columns, preferred_element_type=jnp.float32)
     moves.append(full * (0.01 * scale_ref[0, 2]))
-    half = owners // 2
-    for j in range(base_ref.shape[1] // block):
-        other = me ^ (step * (base_ref.shape[1] // block) + j)
-        for q, masks in enumerate(STREAMS):
-            position = jnp.int32(0)
-            for p in range(owners):
-                position = jnp.where(other == fs_of_position(masks, p), p, position)
-            early, late = held[q]
-            old = jnp.where(position < half, early[position % half], late[position % half])
-            old = old.astype(jnp.float32)
-            near = slice(j * block + q * part, j * block + (q + 1) * part)
-            copy_forget[near] = (old[:part] - moves[0][near]).astype(jnp.bfloat16)
-            copy_value[near] = (old[part : 2 * part] - moves[1][near]).astype(jnp.bfloat16)
-            for h in range(tall // part):
-                down = slice(q * tall + h * part, q * tall + (h + 1) * part)
-                across = slice(j * width, (j + 1) * width)
-                piece = old[2 * part :, h * width : (h + 1) * width]
-                copy_out[down, across] = (piece - moves[2][down, across]).astype(jnp.bfloat16)
+    blocks = base_ref.shape[1] // block
+    for j in range(blocks):
+        owner = step * blocks + j
+        place = (owner - me) % SIDE
+        away = owner // SIDE ^ me // SIDE
+        for t, (near, far) in enumerate(TURNS):
+
+            @pl.when(place // 2 == t)
+            def _(t=t, near=near, far=far):
+                for sources, mask in zip(held[t], (0, near, far, near ^ far)):
+
+                    @pl.when(away == mask)
+                    def _(sources=sources):
+                        if isinstance(sources, tuple):
+                            old_ref[...] = jnp.where(place % 2 == 0, sources[0][0], sources[1][0])
+                        else:
+                            old_ref[...] = sources[place % 2]
+
+        old = old_ref[...].astype(jnp.float32)
+        near = slice(j * block, (j + 1) * block)
+        copy_forget[near] = (old[:block] - moves[0][near]).astype(jnp.bfloat16)
+        copy_value[near] = (old[block : 2 * block] - moves[1][near]).astype(jnp.bfloat16)
+        across = slice(j * width, (j + 1) * width)
+        for h in range(outw_ref.shape[0] // block):
+            down = slice(h * block, (h + 1) * block)
+            piece = old[2 * block :, h * width : (h + 1) * width]
+            copy_out[down, across] = (piece - moves[2][down, across]).astype(jnp.bfloat16)
 
 
 def finish(me, sums, arrived, bases, forget_weight, value_weight, out_weight, held, entries, steps=4):
@@ -207,7 +205,7 @@
     copies.append(jax.ShapeDtypeStruct((out_weight.shape[0], model), jnp.bfloat16))
     down = pl.BlockSpec((tile, columns), lambda i, me: (i, 0))
     across = pl.BlockSpec((out_weight.shape[0], tile), lambda i, me: (0, i))
-    flat = [a for pair in held for a in pair]
+    flat = [a for stream in held for a in stream]
     return pl.pallas_call(
         functools.partial(finish_kernel, entries),
         grid_spec=pltpu.PrefetchScalarGridSpec(
@@ -231,25 +229,37 @@
             scratch_shapes=[
                 pltpu.VMEM((3, rank, columns), jnp.bfloat16),
                 pltpu.VMEM((1, 128), jnp.float32),
+                pltpu.VMEM(flat[0].shape[1:], flat[0].dtype),
             ],
         ),
         out_shape=(*own, *copies, *own),
         compiler_params=LARGE,
         name="finish",
-    )(me[None], sums, arrived, bases, bases, *old, *flat)
-
-
-def swap_all(held, step):
-    owners = lax.axis_size(FS)
-    received = []
-    for masks, value in zip(STREAMS, held):
-        pairs = [(i, i ^ masks[step]) for i in range(owners)]
-        received.append(lax.ppermute(value, FS, pairs))
-    return received
-
-
-def joined(held, received):
-    return [jnp.concatenate(pair) for pair in zip(held, received)]
+    )(me[None], sums, arrived, *[pltpu.with_memory_space_constraint(a, pltpu.HBM) for a in (bases, bases, *old)], *flat)
+
+
+def along(value, away):
+    pairs = [(i, i // SIDE * SIDE + (i - away) % SIDE) for i in range(lax.axis_size(FS))]
+    return lax.ppermute(value, FS, pairs)
+
+
+def passed(value, mask):
+    return lax.ppermute(value, FS, [(i, i ^ mask * SIDE) for i in range(lax.axis_size(FS))])
+
+
+def join_kernel(own_ref, one_ref, two_ref, three_ref, low_ref, high_ref):
+    low_ref[0] = own_ref[0]
+    low_ref[1] = one_ref[0]
+    high_ref[0] = two_ref[0]
+    high_ref[1] = three_ref[0]
+
+
+def joined(*blocks):
+    shape, dtype = blocks[0].shape, blocks[0].dtype
+    pair = jax.ShapeDtypeStruct((2, *shape[1:]), dtype)
+    return pl.pallas_call(
+        join_kernel, out_shape=(pair, pair), compiler_params=SMALL, name="join"
+    )(*blocks)
 
 
 def on_device(
@@ -269,30 +279,28 @@
     me = lax.axis_index(FS).astype(jnp.int32)
     factor = float(normed_input.shape[0] * owners) ** (-0.5)
     rank, columns = bases.shape[2], forget_cot.shape[1]
-    held = list(pack(opening(), forget_weight, value_weight, out_weight))
-    received = swap_all(held, 0)
+    packed = pack(opening(), forget_weight, value_weight, out_weight)
+    one, three, two = (along(packed, away) for away in (1, 3, 2))
+    at_near, at_far = (passed(packed, mask) for mask in (NEAR, FAR))
     inputs = (normed_input, normed_input, output_cot)
     cots = (forget_cot, value_cot, gated_output)
     reduced = [reduced_part(x, bases[k]) for k, x in enumerate(inputs)]
     reduced = lax.optimization_barrier(tuple(reduced))
     parts = [projected_part(r, c, factor) for r, c in zip(reduced, cots)]
     part = jnp.stack([p.reshape(owners, rank // owners, columns) for p in parts], axis=1)
-    held = joined(held, received)
+    held = joined(packed, one, two, three)
     part, *held = lax.optimization_barrier((part, *held))
     arrived = lax.all_to_all(part, FS, split_axis=0, concat_axis=0, tiled=True)
-    received = swap_all(held, 1)
+    nearer = [passed(a, near) for a, (near, _) in zip(held, TURNS)]
+    far_one, near_three = along(at_far, 1), along(at_near, 3)
     moment_one, moment_two, messages = moments(
         arrived, jnp.moveaxis(first_moment, 1, 0), jnp.moveaxis(second_moment, 1, 0)
     )
-    held = joined(held, received)
-    messages, *held = lax.optimization_barrier((messages, *held))
     gathered = lax.all_to_all(messages, FS, split_axis=0, concat_axis=0, tiled=True)
-    received = swap_all(held, 2)
-    sums = squares(gathered)
-    held = joined(held, received)
-    sums, *held = lax.optimization_barrier((sums, *held))
-    received = swap_all(held, 3)
-    sums = lax.all_gather(sums, TP, axis=0)
+    across = [passed(a, far) for a, (_, far) in zip(nearer, TURNS)]
+    near_two = along(near_three, 3)
+    sums = squares(gathered, lax.axis_size(TP))
+    sums = lax.all_to_all(sums, TP, split_axis=0, concat_axis=0, tiled=True)
     entries = float(rank * columns * lax.axis_size(TP))
     finished = finish(
         me,
@@ -302,7 +310,7 @@
         forget_weight,
         value_weight,
         out_weight,
-        list(zip(held, received)),
+        list(zip(held, nearer, (at_far, near_two), (far_one, near_three), across)),
         entries,
     )
     moment_one, moment_two = (jnp.moveaxis(m, 0, 1) for m in (moment_one, moment_two))

time: 78.8 us -> 78.5 us (level)
  the two profiles are of different devices: /device:TPU:1 before, /device:TPU:0 now
where the time goes in v2:
time: 78.5 us; the launch traced here: 77.4 us
  starting transfers between devices  35.4 us (45%)
  waiting for transfers between devices  18.6 us (24%)
  matrix products  10.4 us (13%)
  Pallas kernels  9.99 us (13%)
  local copies, waits for them, and re-layouts  1.14 us (1%)
  between operations  1 us (1%)
  other arithmetic  0.79 us (1%)
    ppermute x6, starting transfers between devices, passed(): lax.ppermute(value, FS, [(i, i ^ mask * SIDE) for i in range(lax.axis_siz...  12.3 us
    ppermute x6, starting transfers between devices, along(): return lax.ppermute(value, FS, pairs)  9.56 us
    dot_general x3, matrix products, reduced_part(): lax.dot_general(basis, x, (((0,), (1,)), ((), ())), preferred_element_typ...  9.12 us
    ppermute x6, waiting for transfers between devices, passed(): lax.ppermute(value, FS, [(i, i ^ mask * SIDE) for i in range(lax.axis_siz...  6.81 us
    pallas_call x1, Pallas kernels, finish(): pl.pallas_call(functools.partial(finish_kernel, entries), grid_spec=pltpu...  6.64 us
    all_to_all x1, waiting for transfers between devices, on_device(): lax.all_to_all(messages, FS, split_axis=0, concat_axis=0, tiled=True)  6.61 us
    all_to_all x1, starting transfers between devices, on_device(): lax.all_to_all(messages, FS, split_axis=0, concat_axis=0, tiled=True)  5.47 us
    all_to_all x1, waiting for transfers between devices, on_device(): sums = lax.all_to_all(sums, TP, split_axis=0, concat_axis=0, tiled=True)  5.2 us
  transfers between devices with their start and end apart: 15, of which 3 were waited for; matrix products, arithmetic and copies ran while one was open for 15% of the time, Pallas kernels for 2%

profile of v2, /device:TPU:0, one launch (start us, length us, event | category | flops | bytes accessed | tf_op | source)
XLA Modules:
  0.0 77.4 jit_solution(7971145651975932498)
XLA Ops:
  0.6 0.0 copy-start
  0.7 0.0 copy-start.3
  0.7 0.0 copy-start.2
  0.7 0.0 copy-start.1
  0.7 0.0 slice-start
  0.7 0.9 %copy-done.3 = f32[256,128]{1,0:T(8,128)S(1)} copy-done((f32[256,128]{1,0:T(8,128)S(1)}, f32[256,128]{1,0:T(8,128)}, u32[]{:S(2)}) %copy-start.3) | copy-done | bytes 131096
  1.7 0.1 copy-done.2
  1.7 0.1 copy-done.1
  1.8 0.7 pack.1.own_ref
  2.5 1.6 %collective-permute-start.2 = (bf16[1,384,256]{2,1,0:T(8,128)(2,1)}, bf16[1,384,256]{2,1,0:T(8,128)(2,1)S(1)}, u32[]{:S(2)}, u32[]{:S(2)}) collective-permute-start(bf16[1,384,256]{2,1,0:T(8,128)(2,1)} %pack.1.own_ref), channel_id=1, source_target_pairs={{0,8},{8,16},{16,24},{24,0},{32,40},{40,48},{48,56},{56,32},{64,72... | collective-permute-start | bytes 589832 | tf_op jit(solution)/shard_map/ppermute | solution.py:243
  4.1 2.7 %collective-permute-start.1 = (bf16[1,384,256]{2,1,0:T(8,128)(2,1)}, bf16[1,384,256]{2,1,0:T(8,128)(2,1)S(1)}, u32[]{:S(2)}, u32[]{:S(2)}) collective-permute-start(bf16[1,384,256]{2,1,0:T(8,128)(2,1)} %pack.1.own_ref), channel_id=1, source_target_pairs={{0,16},{8,24},{16,0},{24,8},{32,48},{40,56},{48,32},{56,40},{64,80... | collective-permute-start | bytes 589832 | tf_op jit(solution)/shard_map/ppermute | solution.py:243
  6.8 1.4 %collective-permute-start = (bf16[1,384,256]{2,1,0:T(8,128)(2,1)}, bf16[1,384,256]{2,1,0:T(8,128)(2,1)S(1)}, u32[]{:S(2)}, u32[]{:S(2)}) collective-permute-start(bf16[1,384,256]{2,1,0:T(8,128)(2,1)} %pack.1.own_ref), channel_id=1, source_target_pairs={{0,24},{8,0},{16,8},{24,16},{32,56},{40,32},{48,40},{56,48},{64,88... | collective-permute-start | bytes 589832 | tf_op jit(solution)/shard_map/ppermute | solution.py:243
  8.3 0.0 slice-start.2
  8.3 3.4 %convolution_convert_fusion.1 = bf16[256,2048]{1,0:T(8,128)(2,1)} fusion(bf16[2048,2048]{1,0:T(8,128)(2,1)S(1)} %bitcast.32, bf16[3,2048,256]{2,1,0:T(8,128)(2,1)S(1)} %copy-done.6), kind=kOutput, calls=%fused_computation.1 | convolution fusion | flops 2148007936 | bytes 10485760 | tf_op jit(solution)/shard_map/dot_general | solution.py:59
  11.6 3.4 %convolution_convert_fusion.2 = bf16[256,2048]{1,0:T(8,128)(2,1)} fusion(bf16[2048,2048]{1,0:T(8,128)(2,1)S(1)} %bitcast.32, bf16[3,2048,256]{2,1,0:T(8,128)(2,1)S(1)} %copy-done.6), kind=kOutput, calls=%fused_computation.2 | convolution fusion | flops 2148007936 | bytes 10485760 | tf_op jit(solution)/shard_map/dot_general | solution.py:59
  15.0 0.0 copy-start.7
  15.0 0.0 copy-start.9
  15.0 0.0 copy-start.8
  15.1 0.0 copy-start.4
  15.1 0.0 copy-start.5
  15.1 2.4 %convolution_convert_fusion = bf16[256,2048]{1,0:T(8,128)(2,1)S(1)} fusion(bf16[2048,2048]{1,0:T(8,128)(2,1)S(1)} %bitcast.34, bf16[3,2048,256]{2,1,0:T(8,128)(2,1)S(1)} %copy-done.6), kind=kOutput, calls=%fused_computation | convolution fusion | flops 2148007936 | bytes 10485760 | tf_op jit(solution)/shard_map/dot_general | solution.py:59
  17.5 0.4 fusion
  18.0 0.4 fusion.1
  18.4 0.4 fusion.2
  18.9 0.8 %pad_maximum_fusion = bf16[16,3,16,256]{3,2,1,0:T(8,128)(2,1)} fusion(bf16[16,1,16,256]{3,2,1,0:T(8,128)(2,1)S(1)} %bitcast.30, bf16[16,1,16,256]{3,2,1,0:T(8,128)(2,1)S(1)} %bitcast.29, bf16[16,1,16,256]{3,2,1,0:T(8,128)(2,1)S(1)} %bitcast.28), kind=kLoop, calls=%fused_computation.15 | loop fusion | flops 393216 | bytes 786432 | tf_op jit(solution)/shard_map/stack | solution.py:290
  19.7 0.0 collective-permute-done.2.three_ref
  19.7 1.0 %join.1 = (bf16[2,384,256]{2,1,0:T(8,128)(2,1)S(1)}, bf16[2,384,256]{2,1,0:T(8,128)(2,1)S(1)}) custom-call(bf16[1,384,256]{2,1,0:T(8,128)(2,1)} %pack.1.own_ref, bf16[1,384,256]{2,1,0:T(8,128)(2,1)S(1)} %collective-permute-done.one_ref, bf16[1,384,256]{2,1,0:T(8,128)(2,1)S(1)} %collective-permute-done.1.two_ref, ...), custom_call_target="tpu_custom_call" | custom-call | tf_op jit(solution)/shard_map/join/pallas_call | solution.py:260
  20.7 2.0 %collective-permute-start.3 = (bf16[2,384,256]{2,1,0:T(8,128)(2,1)S(1)}, bf16[2,384,256]{2,1,0:T(8,128)(2,1)S(1)}, u32[]{:S(2)}, u32[]{:S(2)}) collective-permute-start(bf16[2,384,256]{2,1,0:T(8,128)(2,1)S(1)} %get-tuple-element.38.refs_0_), channel_id=1, source_target_pairs={{0,32},{8,40},{16,48},{24,56},{32,0},{40,8},{48,16},{56,24},{64,96... | collective-permute-start | bytes 1179656 | tf_op jit(solution)/shard_map/ppermute | solution.py:247
  22.6 2.5 %collective-permute-start.7 = (bf16[2,384,256]{2,1,0:T(8,128)(2,1)S(1)}, bf16[2,384,256]{2,1,0:T(8,128)(2,1)S(1)}, u32[]{:S(2)}, u32[]{:S(2)}) collective-permute-start(bf16[2,384,256]{2,1,0:T(8,128)(2,1)S(1)} %get-tuple-element.39.refs_5_), channel_id=1, source_target_pairs={{0,96},{8,104},{16,112},{24,120},{32,64},{40,72},{48,80},{56,88},{... | collective-permute-start | bytes 1179656 | tf_op jit(solution)/shard_map/ppermute | solution.py:247
  25.2 3.6 %all-to-all-start = ((bf16[16,3,16,256]{3,2,1,0:T(8,128)(2,1)}), bf16[16,3,16,256]{3,2,1,0:T(8,128)(2,1)S(1)}, u32[]{:S(2)}, u32[]{:S(2)}) async-start(bf16[16,3,16,256]{3,2,1,0:T(8,128)(2,1)} %pad_maximum_fusion), calls=%async_computation | async-start | bytes 786432 | tf_op jit(solution)/shard_map/all_to_all | solution.py:293
  28.7 1.8 %collective-permute-start.8 = (bf16[1,384,256]{2,1,0:T(8,128)(2,1)}, bf16[1,384,256]{2,1,0:T(8,128)(2,1)}, u32[]{:S(2)}, u32[]{:S(2)}) collective-permute-start(bf16[1,384,256]{2,1,0:T(8,128)(2,1)} %pack.1.own_ref), channel_id=1, source_target_pairs={{0,32},{8,40},{16,48},{24,56},{32,0},{40,8},{48,16},{56,24},{64,96... | collective-permute-start | bytes 589832 | tf_op jit(solution)/shard_map/ppermute | solution.py:247
  30.6 2.1 %collective-permute-start.4 = (bf16[1,384,256]{2,1,0:T(8,128)(2,1)}, bf16[1,384,256]{2,1,0:T(8,128)(2,1)}, u32[]{:S(2)}, u32[]{:S(2)}) collective-permute-start(bf16[1,384,256]{2,1,0:T(8,128)(2,1)} %pack.1.own_ref), channel_id=1, source_target_pairs={{0,96},{8,104},{16,112},{24,120},{32,64},{40,72},{48,80},{56,88},{... | collective-permute-start | bytes 589832 | tf_op jit(solution)/shard_map/ppermute | solution.py:247
  32.7 6.8 %collective-permute-done.8 = bf16[1,384,256]{2,1,0:T(8,128)(2,1)} collective-permute-done((bf16[1,384,256]{2,1,0:T(8,128)(2,1)}, bf16[1,384,256]{2,1,0:T(8,128)(2,1)}, u32[]{:S(2)}, u32[]{:S(2)}) %collective-permute-start.8) | collective-permute-done | bytes 196640 | tf_op jit(solution)/shard_map/ppermute | solution.py:247
  39.5 0.6 collective-permute-start.9
  40.0 0.0 collective-permute-done.3.refs_1_
  40.1 3.9 %collective-permute-start.6 = (bf16[2,384,256]{2,1,0:T(8,128)(2,1)S(1)}, bf16[2,384,256]{2,1,0:T(8,128)(2,1)S(1)}, u32[]{:S(2)}, u32[]{:S(2)}) collective-permute-start(bf16[2,384,256]{2,1,0:T(8,128)(2,1)S(1)} %collective-permute-done.3.refs_1_), channel_id=1, source_target_pairs={{0,96},{8,104},{16,112},{24,120},{32,64},{40,72},{48,80},{56,88},{... | collective-permute-start | bytes 1179656 | tf_op jit(solution)/shard_map/ppermute | solution.py:247
  43.9 0.0 collective-permute-done.7.refs_6_
  43.9 0.0 collective-permute-start.11
  43.9 0.0 all-to-all-done.arrived_ref
  43.9 0.9 %moments.1 = (f32[3,16,256]{2,1,0:T(8,128)}, f32[3,16,256]{2,1,0:T(8,128)}, bf16[16,48,256]{2,1,0:T(8,128)(2,1)}) custom-call(bf16[16,3,16,256]{3,2,1,0:T(8,128)(2,1)S(1)} %all-to-all-done.arrived_ref, f32[3,16,256]{2,1,0:T(8,128)S(1)} %bitcast.26, f32[3,16,256]{2,1,0:T(8,128)S(1)} %bitcast.27), custom_call_target="tpu_custom_call" | custom-call | tf_op jit(solution)/shard_map/moments/pallas_call | solution.py:87
  44.8 5.5 %all-to-all-start.1 = ((bf16[16,48,256]{2,1,0:T(8,128)(2,1)}), bf16[16,48,256]{2,1,0:T(8,128)(2,1)S(1)}, u32[]{:S(2)}, u32[]{:S(2)}) async-start(bf16[16,48,256]{2,1,0:T(8,128)(2,1)} %get-tuple-element.37), calls=%async_computation.1 | async-start | bytes 786432 | tf_op jit(solution)/shard_map/all_to_all | solution.py:299
  50.3 3.2 %collective-permute-start.5 = (bf16[1,384,256]{2,1,0:T(8,128)(2,1)}, bf16[1,384,256]{2,1,0:T(8,128)(2,1)}, u32[]{:S(2)}, u32[]{:S(2)}) collective-permute-start(bf16[1,384,256]{2,1,0:T(8,128)(2,1)} %collective-permute-done.4.refs_2_), channel_id=1, source_target_pairs={{0,24},{8,0},{16,8},{24,16},{32,56},{40,32},{48,40},{56,48},{64,88... | collective-permute-start | bytes 589832 | tf_op jit(solution)/shard_map/ppermute | solution.py:243
  53.5 0.0 collective-permute-done.9.refs_8_
  53.5 6.6 %all-to-all-done.1.arrived_ref = bf16[16,48,256]{2,1,0:T(8,128)(2,1)S(1)} async-done(((bf16[16,48,256]{2,1,0:T(8,128)(2,1)}), bf16[16,48,256]{2,1,0:T(8,128)(2,1)S(1)}, u32[]{:S(2)}, u32[]{:S(2)}) %all-to-all-start.1) | async-done | bytes 393248 | tf_op jit(solution)/shard_map/all_to_all | solution.py:299
  60.1 0.8 %squares.1 = f32[8,1,128]{2,1,0:T(1,128)} custom-call(bf16[16,48,256]{2,1,0:T(8,128)(2,1)S(1)} %all-to-all-done.1.arrived_ref), custom_call_target="tpu_custom_call" | custom-call | tf_op jit(solution)/shard_map/squares/pallas_call | solution.py:106
  60.9 4.5 %all-to-all-start.2 = ((f32[8,1,128]{2,1,0:T(1,128)}), f32[8,1,128]{2,1,0:T(1,128)S(1)}, u32[]{:S(2)}, u32[]{:S(2)}) async-start(f32[8,1,128]{2,1,0:T(1,128)} %squares.1), calls=%async_computation.2 | async-start | bytes 8192 | tf_op jit(solution)/shard_map/all_to_all | solution.py:303
  65.4 5.2 %all-to-all-done.2.sums_ref = f32[8,1,128]{2,1,0:T(1,128)S(1)} async-done(((f32[8,1,128]{2,1,0:T(1,128)}), f32[8,1,128]{2,1,0:T(1,128)S(1)}, u32[]{:S(2)}, u32[]{:S(2)}) %all-to-all-start.2) | async-done | bytes 4128 | tf_op jit(solution)/shard_map/all_to_all | solution.py:303
  70.6 6.6 %finish.1 = (f32[128,256]{1,0:T(8,128)}, f32[128,256]{1,0:T(8,128)}, f32[256,128]{1,0:T(8,128)}, bf16[2048,256]{1,0:T(8,128)(2,1)}, bf16[2048,256]{1,0:T(8,128)(...) custom-call(s32[1]{0:T(128)} %bitcast.me_ref, ...), custom_call_target="tpu_custom_call" | custom-call | tf_op jit(solution)/shard_map/finish/pallas_call | solution.py:209
  (27 shorter events, 0.1 us)
Async XLA Ops:
  0.6 16.8 %copy-start = (bf16[2048,256]{1,0:T(8,128)(2,1)S(1)}, bf16[2048,256]{1,0:T(8,128)(2,1)}, u32[]{:S(2)}) copy-start(bf16[2048,256]{1,0:T(8,128)(2,1)} %param.12) | copy-start | bytes 3145732
  0.7 1.0 %copy-start.3 = (f32[256,128]{1,0:T(8,128)S(1)}, f32[256,128]{1,0:T(8,128)}, u32[]{:S(2)}) copy-start(f32[256,128]{1,0:T(8,128)} %outw_ref.1) | copy-start | bytes 393220
  0.7 1.0 %copy-start.2 = (f32[128,256]{1,0:T(8,128)S(1)}, f32[128,256]{1,0:T(8,128)}, u32[]{:S(2)}) copy-start(f32[128,256]{1,0:T(8,128)} %value_ref.3) | copy-start | bytes 393220
  0.7 1.1 %copy-start.1 = (f32[128,256]{1,0:T(8,128)S(1)}, f32[128,256]{1,0:T(8,128)}, u32[]{:S(2)}) copy-start(f32[128,256]{1,0:T(8,128)} %forget_ref.3) | copy-start | bytes 393220
  0.7 7.6 %slice-start = ((s8[8388608]{0:T(1024)(128)(4,1)}), s8[4194304]{0:T(1024)(128)(4,1)S(1)}, s32[]{:S(2)}) async-start(s8[8388608]{0:T(1024)(128)(4,1)} %bitcast.31), calls=%async_computation.3 | async-start | bytes 8388608
  1.8 6.5 %copy-start.6 = (bf16[3,2048,256]{2,1,0:T(8,128)(2,1)S(1)}, bf16[3,2048,256]{2,1,0:T(8,128)(2,1)}, u32[]{:S(2)}) copy-start(bf16[3,2048,256]{2,1,0:T(8,128)(2,1)} %mine_ref.1) | copy-start | bytes 9437188
  1.8 6.5 %slice-start.1 = ((s8[8388608]{0:T(1024)(128)(4,1)}), s8[4194304]{0:T(1024)(128)(4,1)S(1)}, s32[]{:S(2)}) async-start(s8[8388608]{0:T(1024)(128)(4,1)} %bitcast.31), calls=%async_computation.4 | async-start | bytes 8388608
  2.5 17.2 %collective-permute-start.2 = (bf16[1,384,256]{2,1,0:T(8,128)(2,1)}, bf16[1,384,256]{2,1,0:T(8,128)(2,1)S(1)}, u32[]{:S(2)}, u32[]{:S(2)}) collective-permute-start(bf16[1,384,256]{2,1,0:T(8,128)(2,1)} %pack.1.own_ref), channel_id=1, source_target_pairs={{0,8},{8,16},{16,24},{24,0},{32,40},{40,48},{48,56},{56,32},{64,72... | collective-permute-start | bytes 589832 | tf_op jit(solution)/shard_map/ppermute | solution.py:243
  4.1 15.6 %collective-permute-start.1 = (bf16[1,384,256]{2,1,0:T(8,128)(2,1)}, bf16[1,384,256]{2,1,0:T(8,128)(2,1)S(1)}, u32[]{:S(2)}, u32[]{:S(2)}) collective-permute-start(bf16[1,384,256]{2,1,0:T(8,128)(2,1)} %pack.1.own_ref), channel_id=1, source_target_pairs={{0,16},{8,24},{16,0},{24,8},{32,48},{40,56},{48,32},{56,40},{64,80... | collective-permute-start | bytes 589832 | tf_op jit(solution)/shard_map/ppermute | solution.py:243
  6.8 12.8 %collective-permute-start = (bf16[1,384,256]{2,1,0:T(8,128)(2,1)}, bf16[1,384,256]{2,1,0:T(8,128)(2,1)S(1)}, u32[]{:S(2)}, u32[]{:S(2)}) collective-permute-start(bf16[1,384,256]{2,1,0:T(8,128)(2,1)} %pack.1.own_ref), channel_id=1, source_target_pairs={{0,24},{8,0},{16,8},{24,16},{32,56},{40,32},{48,40},{56,48},{64,88... | collective-permute-start | bytes 589832 | tf_op jit(solution)/shard_map/ppermute | solution.py:243
  8.3 6.7 %slice-start.2 = ((s8[8388608]{0:T(1024)(128)(4,1)}), s8[4194304]{0:T(1024)(128)(4,1)S(1)}, s32[]{:S(2)}) async-start(s8[8388608]{0:T(1024)(128)(4,1)} %bitcast.33), calls=%async_computation.5 | async-start | bytes 8388608
  11.6 3.4 %slice-start.3 = ((s8[8388608]{0:T(1024)(128)(4,1)}), s8[4194304]{0:T(1024)(128)(4,1)S(1)}, s32[]{:S(2)}) async-start(s8[8388608]{0:T(1024)(128)(4,1)} %bitcast.33), calls=%async_computation.6 | async-start | bytes 8388608
  15.0 2.5 %copy-start.10 = (bf16[256,2048]{1,0:T(8,128)(2,1)S(1)}, bf16[256,2048]{1,0:T(8,128)(2,1)}, u32[]{:S(2)}) copy-start(bf16[256,2048]{1,0:T(8,128)(2,1)} %convolution_convert_fusion.2) | copy-start | bytes 3145732
  15.0 2.9 %copy-start.7 = (bf16[2048,256]{1,0:T(8,128)(2,1)S(1)}, bf16[2048,256]{1,0:T(8,128)(2,1)}, u32[]{:S(2)}) copy-start(bf16[2048,256]{1,0:T(8,128)(2,1)} %param.13) | copy-start | bytes 3145732
  15.0 2.9 %copy-start.9 = (bf16[256,2048]{1,0:T(8,128)(2,1)S(1)}, bf16[256,2048]{1,0:T(8,128)(2,1)}, u32[]{:S(2)}) copy-start(bf16[256,2048]{1,0:T(8,128)(2,1)} %convolution_convert_fusion.1) | copy-start | bytes 3145732
  15.0 3.4 %copy-start.8 = (bf16[2048,256]{1,0:T(8,128)(2,1)S(1)}, bf16[2048,256]{1,0:T(8,128)(2,1)}, u32[]{:S(2)}) copy-start(bf16[2048,256]{1,0:T(8,128)(2,1)} %param.14) | copy-start | bytes 3145732
  15.1 28.9 %copy-start.4 = (f32[16,3,256]{2,0,1:T(8,128)S(1)}, f32[16,3,256]{2,0,1:T(8,128)}, u32[]{:S(2)}) copy-start(f32[16,3,256]{2,0,1:T(8,128)} %param.20) | copy-start | bytes 147460
  15.1 28.9 %copy-start.5 = (f32[16,3,256]{2,0,1:T(8,128)S(1)}, f32[16,3,256]{2,0,1:T(8,128)}, u32[]{:S(2)}) copy-start(f32[16,3,256]{2,0,1:T(8,128)} %param.21) | copy-start | bytes 147460
  20.7 19.4 %collective-permute-start.3 = (bf16[2,384,256]{2,1,0:T(8,128)(2,1)S(1)}, bf16[2,384,256]{2,1,0:T(8,128)(2,1)S(1)}, u32[]{:S(2)}, u32[]{:S(2)}) collective-permute-start(bf16[2,384,256]{2,1,0:T(8,128)(2,1)S(1)} %get-tuple-element.38.refs_0_), channel_id=1, source_target_pairs={{0,32},{8,40},{16,48},{24,56},{32,0},{40,8},{48,16},{56,24},{64,96... | collective-permute-start | bytes 1179656 | tf_op jit(solution)/shard_map/ppermute | solution.py:247
  22.6 21.3 %collective-permute-start.7 = (bf16[2,384,256]{2,1,0:T(8,128)(2,1)S(1)}, bf16[2,384,256]{2,1,0:T(8,128)(2,1)S(1)}, u32[]{:S(2)}, u32[]{:S(2)}) collective-permute-start(bf16[2,384,256]{2,1,0:T(8,128)(2,1)S(1)} %get-tuple-element.39.refs_5_), channel_id=1, source_target_pairs={{0,96},{8,104},{16,112},{24,120},{32,64},{40,72},{48,80},{56,88},{... | collective-permute-start | bytes 1179656 | tf_op jit(solution)/shard_map/ppermute | solution.py:247
  25.2 18.7 %all-to-all-start = ((bf16[16,3,16,256]{3,2,1,0:T(8,128)(2,1)}), bf16[16,3,16,256]{3,2,1,0:T(8,128)(2,1)S(1)}, u32[]{:S(2)}, u32[]{:S(2)}) async-start(bf16[16,3,16,256]{3,2,1,0:T(8,128)(2,1)} %pad_maximum_fusion), calls=%async_computation | async-start | bytes 786432 | tf_op jit(solution)/shard_map/all_to_all | solution.py:293
  28.7 10.7 %collective-permute-start.8 = (bf16[1,384,256]{2,1,0:T(8,128)(2,1)}, bf16[1,384,256]{2,1,0:T(8,128)(2,1)}, u32[]{:S(2)}, u32[]{:S(2)}) collective-permute-start(bf16[1,384,256]{2,1,0:T(8,128)(2,1)} %pack.1.own_ref), channel_id=1, source_target_pairs={{0,32},{8,40},{16,48},{24,56},{32,0},{40,8},{48,16},{56,24},{64,96... | collective-permute-start | bytes 589832 | tf_op jit(solution)/shard_map/ppermute | solution.py:247
  30.6 19.7 %collective-permute-start.4 = (bf16[1,384,256]{2,1,0:T(8,128)(2,1)}, bf16[1,384,256]{2,1,0:T(8,128)(2,1)}, u32[]{:S(2)}, u32[]{:S(2)}) collective-permute-start(bf16[1,384,256]{2,1,0:T(8,128)(2,1)} %pack.1.own_ref), channel_id=1, source_target_pairs={{0,96},{8,104},{16,112},{24,120},{32,64},{40,72},{48,80},{56,88},{... | collective-permute-start | bytes 589832 | tf_op jit(solution)/shard_map/ppermute | solution.py:247
  39.5 14.0 %collective-permute-start.9 = (bf16[1,384,256]{2,1,0:T(8,128)(2,1)}, bf16[1,384,256]{2,1,0:T(8,128)(2,1)}, u32[]{:S(2)}, u32[]{:S(2)}) collective-permute-start(bf16[1,384,256]{2,1,0:T(8,128)(2,1)} %collective-permute-done.8), channel_id=1, source_target_pairs={{0,8},{8,16},{16,24},{24,0},{32,40},{40,48},{48,56},{56,32},{64,72... | collective-permute-start | bytes 589832 | tf_op jit(solution)/shard_map/ppermute | solution.py:243
  40.1 30.6 %collective-permute-start.6 = (bf16[2,384,256]{2,1,0:T(8,128)(2,1)S(1)}, bf16[2,384,256]{2,1,0:T(8,128)(2,1)S(1)}, u32[]{:S(2)}, u32[]{:S(2)}) collective-permute-start(bf16[2,384,256]{2,1,0:T(8,128)(2,1)S(1)} %collective-permute-done.3.refs_1_), channel_id=1, source_target_pairs={{0,96},{8,104},{16,112},{24,120},{32,64},{40,72},{48,80},{56,88},{... | collective-permute-start | bytes 1179656 | tf_op jit(solution)/shard_map/ppermute | solution.py:247
  43.9 26.7 %collective-permute-start.11 = (bf16[2,384,256]{2,1,0:T(8,128)(2,1)S(1)}, bf16[2,384,256]{2,1,0:T(8,128)(2,1)}, u32[]{:S(2)}, u32[]{:S(2)}) collective-permute-start(bf16[2,384,256]{2,1,0:T(8,128)(2,1)S(1)} %collective-permute-done.7.refs_6_), channel_id=1, source_target_pairs={{0,32},{8,40},{16,48},{24,56},{32,0},{40,8},{48,16},{56,24},{64,96... | collective-permute-start | bytes 1179656 | tf_op jit(solution)/shard_map/ppermute | solution.py:247
  44.8 15.3 %all-to-all-start.1 = ((bf16[16,48,256]{2,1,0:T(8,128)(2,1)}), bf16[16,48,256]{2,1,0:T(8,128)(2,1)S(1)}, u32[]{:S(2)}, u32[]{:S(2)}) async-start(bf16[16,48,256]{2,1,0:T(8,128)(2,1)} %get-tuple-element.37), calls=%async_computation.1 | async-start | bytes 786432 | tf_op jit(solution)/shard_map/all_to_all | solution.py:299
  50.3 15.1 %collective-permute-start.5 = (bf16[1,384,256]{2,1,0:T(8,128)(2,1)}, bf16[1,384,256]{2,1,0:T(8,128)(2,1)}, u32[]{:S(2)}, u32[]{:S(2)}) collective-permute-start(bf16[1,384,256]{2,1,0:T(8,128)(2,1)} %collective-permute-done.4.refs_2_), channel_id=1, source_target_pairs={{0,24},{8,0},{16,8},{24,16},{32,56},{40,32},{48,40},{56,48},{64,88... | collective-permute-start | bytes 589832 | tf_op jit(solution)/shard_map/ppermute | solution.py:243
  53.5 11.9 %collective-permute-start.10 = (bf16[1,384,256]{2,1,0:T(8,128)(2,1)}, bf16[1,384,256]{2,1,0:T(8,128)(2,1)}, u32[]{:S(2)}, u32[]{:S(2)}) collective-permute-start(bf16[1,384,256]{2,1,0:T(8,128)(2,1)} %collective-permute-done.9.refs_8_), channel_id=1, source_target_pairs={{0,8},{8,16},{16,24},{24,0},{32,40},{40,48},{48,56},{56,32},{64,72... | collective-permute-start | bytes 589832 | tf_op jit(solution)/shard_map/ppermute | solution.py:243
  60.9 9.7 %all-to-all-start.2 = ((f32[8,1,128]{2,1,0:T(1,128)}), f32[8,1,128]{2,1,0:T(1,128)S(1)}, u32[]{:S(2)}, u32[]{:S(2)}) async-start(f32[8,1,128]{2,1,0:T(1,128)} %squares.1), calls=%async_computation.2 | async-start | bytes 8192 | tf_op jit(solution)/shard_map/all_to_all | solution.py:303

commit v3 on v2

--- a/solution.py
+++ b/solution.py
@@ -194,7 +194,7 @@
             copy_out[down, across] = (piece - moves[2][down, across]).astype(jnp.bfloat16)
 
 
-def finish(me, sums, arrived, bases, forget_weight, value_weight, out_weight, held, entries, steps=4):
+def finish(me, sums, arrived, bases, forget_weight, value_weight, out_weight, held, entries, steps=2):
     block, columns = forget_weight.shape
     model, rank = bases.shape[1:]
     tile = model // steps
@@ -284,9 +284,11 @@
     at_near, at_far = (passed(packed, mask) for mask in (NEAR, FAR))
     inputs = (normed_input, normed_input, output_cot)
     cots = (forget_cot, value_cot, gated_output)
-    reduced = [reduced_part(x, bases[k]) for k, x in enumerate(inputs)]
-    reduced = lax.optimization_barrier(tuple(reduced))
-    parts = [projected_part(r, c, factor) for r, c in zip(reduced, cots)]
+    parts = []
+    for k, (x, cot) in enumerate(zip(inputs, cots)):
+        x, parts = lax.optimization_barrier((x, parts))
+        reduced = reduced_part(x, bases[k])
+        parts.append(projected_part(lax.optimization_barrier(reduced), cot, factor))
     part = jnp.stack([p.reshape(owners, rank // owners, columns) for p in parts], axis=1)
     held = joined(packed, one, two, three)
     part, *held = lax.optimization_barrier((part, *held))

time: 78.5 us -> 76.2 us (0.971)
  matrix products: 10.4 us -> 8.49 us
    dot_general x3, matrix products: 9.12 us -> 7.08 us  [reduced_part(): lax.dot_general(basis, x, (((0,), (1,)), ((), ())), preferred_element_typ...]
    unnamed x30 -> x26, local copies, waits for them, and re-layouts: 1.14 us -> 1.6 us
  transfers between devices with their start and end apart: 15 -> 15, of which waited for: 3 -> 3; matrix products, arithmetic and copies ran while one was open for 15% -> 12% of each run, Pallas kernels for 2% -> 2%
where the time goes in v3:
time: 76.2 us; the launch traced here: 75.2 us
  starting transfers between devices  35.4 us (46%)
  waiting for transfers between devices  18.6 us (24%)
  Pallas kernels  9.33 us (12%)
  matrix products  8.49 us (11%)
  local copies, waits for them, and re-layouts  1.6 us (2%)
  between operations  0.93 us (1%)
  other arithmetic  0.79 us (1%)
    ppermute x6, starting transfers between devices, passed(): lax.ppermute(value, FS, [(i, i ^ mask * SIDE) for i in range(lax.axis_siz...  12.3 us
    ppermute x6, starting transfers between devices, along(): return lax.ppermute(value, FS, pairs)  9.57 us
    dot_general x3, matrix products, reduced_part(): lax.dot_general(basis, x, (((0,), (1,)), ((), ())), preferred_element_typ...  7.08 us
    ppermute x6, waiting for transfers between devices, passed(): lax.ppermute(value, FS, [(i, i ^ mask * SIDE) for i in range(lax.axis_siz...  6.81 us
    all_to_all x1, waiting for transfers between devices, on_device(): lax.all_to_all(messages, FS, split_axis=0, concat_axis=0, tiled=True)  6.61 us
    pallas_call x1, Pallas kernels, finish(): pl.pallas_call(functools.partial(finish_kernel, entries), grid_spec=pltpu...  5.98 us
    all_to_all x1, starting transfers between devices, on_device(): lax.all_to_all(messages, FS, split_axis=0, concat_axis=0, tiled=True)  5.47 us
    all_to_all x1, waiting for transfers between devices, on_device(): sums = lax.all_to_all(sums, TP, split_axis=0, concat_axis=0, tiled=True)  5.2 us
  transfers between devices with their start and end apart: 15, of which 3 were waited for; matrix products, arithmetic and copies ran while one was open for 12% of the time, Pallas kernels for 2%

profile of v3, /device:TPU:0, one launch (start us, length us, event | category | flops | bytes accessed | tf_op | source)
XLA Modules:
  0.0 75.2 jit_solution(4779952082346628072)
XLA Ops:
  0.6 0.0 copy-start
  0.7 0.0 copy-start.3
  0.7 0.0 copy-start.2
  0.7 0.0 copy-start.1
  0.7 0.0 slice-start
  0.7 0.9 %copy-done.3 = f32[256,128]{1,0:T(8,128)S(1)} copy-done((f32[256,128]{1,0:T(8,128)S(1)}, f32[256,128]{1,0:T(8,128)}, u32[]{:S(2)}) %copy-start.3) | copy-done | bytes 131096
  1.7 0.1 copy-done.2
  1.7 0.1 copy-done.1
  1.8 0.7 pack.1.own_ref
  2.5 1.6 %collective-permute-start.2 = (bf16[1,384,256]{2,1,0:T(8,128)(2,1)}, bf16[1,384,256]{2,1,0:T(8,128)(2,1)S(1)}, u32[]{:S(2)}, u32[]{:S(2)}) collective-permute-start(bf16[1,384,256]{2,1,0:T(8,128)(2,1)} %pack.1.own_ref), channel_id=1, source_target_pairs={{0,8},{8,16},{16,24},{24,0},{32,40},{40,48},{48,56},{56,32},{64,72... | collective-permute-start | bytes 589832 | tf_op jit(solution)/shard_map/ppermute | solution.py:243
  4.1 2.7 %collective-permute-start.1 = (bf16[1,384,256]{2,1,0:T(8,128)(2,1)}, bf16[1,384,256]{2,1,0:T(8,128)(2,1)S(1)}, u32[]{:S(2)}, u32[]{:S(2)}) collective-permute-start(bf16[1,384,256]{2,1,0:T(8,128)(2,1)} %pack.1.own_ref), channel_id=1, source_target_pairs={{0,16},{8,24},{16,0},{24,8},{32,48},{40,56},{48,32},{56,40},{64,80... | collective-permute-start | bytes 589832 | tf_op jit(solution)/shard_map/ppermute | solution.py:243
  6.8 1.4 %collective-permute-start = (bf16[1,384,256]{2,1,0:T(8,128)(2,1)}, bf16[1,384,256]{2,1,0:T(8,128)(2,1)S(1)}, u32[]{:S(2)}, u32[]{:S(2)}) collective-permute-start(bf16[1,384,256]{2,1,0:T(8,128)(2,1)} %pack.1.own_ref), channel_id=1, source_target_pairs={{0,24},{8,0},{16,8},{24,16},{32,56},{40,32},{48,40},{56,48},{64,88... | collective-permute-start | bytes 589832 | tf_op jit(solution)/shard_map/ppermute | solution.py:243
  8.3 2.4 %convolution_convert_fusion.2 = bf16[256,2048]{1,0:T(8,128)(2,1)S(1)} fusion(bf16[2048,2048]{1,0:T(8,128)(2,1)S(1)} %bitcast.36, bf16[3,2048,256]{2,1,0:T(8,128)(2,1)S(1)} %copy-done.6), kind=kOutput, calls=%fused_computation.2 | convolution fusion | flops 2148007936 | bytes 10485760 | tf_op jit(solution)/shard_map/dot_general | solution.py:59
  10.7 0.0 slice-start.2
  10.7 0.4 fusion.2
  11.1 0.0 copy-start.7
  11.1 0.0 slice-start.3
  11.2 2.3 %fusion = bf16[256,2048]{0,1:T(8,128)(2,1)S(1)} fusion(bf16[2048,2048]{1,0:T(8,128)(2,1)S(1)} %bitcast.36, bf16[3,2048,256]{2,1,0:T(8,128)(2,1)S(1)} %copy-done.6), kind=kOutput, calls=%fused_computation.3 | convolution fusion | flops 2148007936 | bytes 10485760 | tf_op jit(solution)/shard_map/dot_general | solution.py:59
  13.5 0.5 fusion.3
  14.0 0.5 slice-done.3
  14.5 2.3 %fusion.1 = bf16[256,2048]{0,1:T(8,128)(2,1)S(1)} fusion(bf16[2048,2048]{1,0:T(8,128)(2,1)S(1)} %bitcast.38, bf16[3,2048,256]{2,1,0:T(8,128)(2,1)S(1)} %copy-done.6), kind=kOutput, calls=%fused_computation.4 | convolution fusion | flops 2148007936 | bytes 10485760 | tf_op jit(solution)/shard_map/dot_general | solution.py:59
  16.9 0.5 fusion.4
  17.4 0.8 %pad_maximum_fusion = bf16[16,3,16,256]{3,2,1,0:T(8,128)(2,1)} fusion(bf16[16,1,16,256]{3,2,1,0:T(8,128)(2,1)S(1)} %bitcast.33, bf16[16,1,16,256]{3,2,1,0:T(8,128)(2,1)S(1)} %bitcast.32, bf16[16,1,16,256]{3,2,1,0:T(8,128)(2,1)S(1)} %bitcast.34), kind=kLoop, calls=%fused_computation.17 | loop fusion | flops 393216 | bytes 786432 | tf_op jit(solution)/shard_map/stack | solution.py:292
  18.1 0.0 collective-permute-done.2.three_ref
  18.1 0.0 collective-permute-done.1.two_ref
  18.2 0.0 collective-permute-done.one_ref
  18.2 1.0 %join.1 = (bf16[2,384,256]{2,1,0:T(8,128)(2,1)S(1)}, bf16[2,384,256]{2,1,0:T(8,128)(2,1)S(1)}) custom-call(bf16[1,384,256]{2,1,0:T(8,128)(2,1)} %pack.1.own_ref, bf16[1,384,256]{2,1,0:T(8,128)(2,1)S(1)} %collective-permute-done.one_ref, bf16[1,384,256]{2,1,0:T(8,128)(2,1)S(1)} %collective-permute-done.1.two_ref, ...), custom_call_target="tpu_custom_call" | custom-call | tf_op jit(solution)/shard_map/join/pallas_call | solution.py:260
  19.1 2.0 %collective-permute-start.3 = (bf16[2,384,256]{2,1,0:T(8,128)(2,1)S(1)}, bf16[2,384,256]{2,1,0:T(8,128)(2,1)S(1)}, u32[]{:S(2)}, u32[]{:S(2)}) collective-permute-start(bf16[2,384,256]{2,1,0:T(8,128)(2,1)S(1)} %get-tuple-element.42.refs_0_), channel_id=1, source_target_pairs={{0,32},{8,40},{16,48},{24,56},{32,0},{40,8},{48,16},{56,24},{64,96... | collective-permute-start | bytes 1179656 | tf_op jit(solution)/shard_map/ppermute | solution.py:247
  21.1 2.5 %collective-permute-start.7 = (bf16[2,384,256]{2,1,0:T(8,128)(2,1)S(1)}, bf16[2,384,256]{2,1,0:T(8,128)(2,1)S(1)}, u32[]{:S(2)}, u32[]{:S(2)}) collective-permute-start(bf16[2,384,256]{2,1,0:T(8,128)(2,1)S(1)} %get-tuple-element.43.refs_5_), channel_id=1, source_target_pairs={{0,96},{8,104},{16,112},{24,120},{32,64},{40,72},{48,80},{56,88},{... | collective-permute-start | bytes 1179656 | tf_op jit(solution)/shard_map/ppermute | solution.py:247
  23.7 3.6 %all-to-all-start = ((bf16[16,3,16,256]{3,2,1,0:T(8,128)(2,1)}), bf16[16,3,16,256]{3,2,1,0:T(8,128)(2,1)S(1)}, u32[]{:S(2)}, u32[]{:S(2)}) async-start(bf16[16,3,16,256]{3,2,1,0:T(8,128)(2,1)} %pad_maximum_fusion), calls=%async_computation | async-start | bytes 786432 | tf_op jit(solution)/shard_map/all_to_all | solution.py:295
  27.2 1.8 %collective-permute-start.8 = (bf16[1,384,256]{2,1,0:T(8,128)(2,1)}, bf16[1,384,256]{2,1,0:T(8,128)(2,1)}, u32[]{:S(2)}, u32[]{:S(2)}) collective-permute-start(bf16[1,384,256]{2,1,0:T(8,128)(2,1)} %pack.1.own_ref), channel_id=1, source_target_pairs={{0,32},{8,40},{16,48},{24,56},{32,0},{40,8},{48,16},{56,24},{64,96... | collective-permute-start | bytes 589832 | tf_op jit(solution)/shard_map/ppermute | solution.py:247
  29.1 2.1 %collective-permute-start.4 = (bf16[1,384,256]{2,1,0:T(8,128)(2,1)}, bf16[1,384,256]{2,1,0:T(8,128)(2,1)}, u32[]{:S(2)}, u32[]{:S(2)}) collective-permute-start(bf16[1,384,256]{2,1,0:T(8,128)(2,1)} %pack.1.own_ref), channel_id=1, source_target_pairs={{0,96},{8,104},{16,112},{24,120},{32,64},{40,72},{48,80},{56,88},{... | collective-permute-start | bytes 589832 | tf_op jit(solution)/shard_map/ppermute | solution.py:247
  31.1 6.8 %collective-permute-done.8 = bf16[1,384,256]{2,1,0:T(8,128)(2,1)} collective-permute-done((bf16[1,384,256]{2,1,0:T(8,128)(2,1)}, bf16[1,384,256]{2,1,0:T(8,128)(2,1)}, u32[]{:S(2)}, u32[]{:S(2)}) %collective-permute-start.8) | collective-permute-done | bytes 196640 | tf_op jit(solution)/shard_map/ppermute | solution.py:247
  37.9 0.6 collective-permute-start.9
  38.5 0.0 collective-permute-done.3.refs_1_
  38.5 3.9 %collective-permute-start.6 = (bf16[2,384,256]{2,1,0:T(8,128)(2,1)S(1)}, bf16[2,384,256]{2,1,0:T(8,128)(2,1)S(1)}, u32[]{:S(2)}, u32[]{:S(2)}) collective-permute-start(bf16[2,384,256]{2,1,0:T(8,128)(2,1)S(1)} %collective-permute-done.3.refs_1_), channel_id=1, source_target_pairs={{0,96},{8,104},{16,112},{24,120},{32,64},{40,72},{48,80},{56,88},{... | collective-permute-start | bytes 1179656 | tf_op jit(solution)/shard_map/ppermute | solution.py:247
  42.4 0.0 collective-permute-done.7.refs_6_
  42.4 0.0 collective-permute-start.11
  42.4 0.0 all-to-all-done.arrived_ref
  42.4 0.9 %moments.1 = (f32[3,16,256]{2,1,0:T(8,128)}, f32[3,16,256]{2,1,0:T(8,128)}, bf16[16,48,256]{2,1,0:T(8,128)(2,1)}) custom-call(bf16[16,3,16,256]{3,2,1,0:T(8,128)(2,1)S(1)} %all-to-all-done.arrived_ref, f32[3,16,256]{2,1,0:T(8,128)S(1)} %bitcast.30, f32[3,16,256]{2,1,0:T(8,128)S(1)} %bitcast.31), custom_call_target="tpu_custom_call" | custom-call | tf_op jit(solution)/shard_map/moments/pallas_call | solution.py:87
  43.3 5.5 %all-to-all-start.1 = ((bf16[16,48,256]{2,1,0:T(8,128)(2,1)}), bf16[16,48,256]{2,1,0:T(8,128)(2,1)S(1)}, u32[]{:S(2)}, u32[]{:S(2)}) async-start(bf16[16,48,256]{2,1,0:T(8,128)(2,1)} %get-tuple-element.41), calls=%async_computation.1 | async-start | bytes 786432 | tf_op jit(solution)/shard_map/all_to_all | solution.py:301
  48.8 3.2 %collective-permute-start.5 = (bf16[1,384,256]{2,1,0:T(8,128)(2,1)}, bf16[1,384,256]{2,1,0:T(8,128)(2,1)}, u32[]{:S(2)}, u32[]{:S(2)}) collective-permute-start(bf16[1,384,256]{2,1,0:T(8,128)(2,1)} %collective-permute-done.4.refs_2_), channel_id=1, source_target_pairs={{0,24},{8,0},{16,8},{24,16},{32,56},{40,32},{48,40},{56,48},{64,88... | collective-permute-start | bytes 589832 | tf_op jit(solution)/shard_map/ppermute | solution.py:243
  52.0 0.0 collective-permute-done.9.refs_8_
  52.0 6.6 %all-to-all-done.1.arrived_ref = bf16[16,48,256]{2,1,0:T(8,128)(2,1)S(1)} async-done(((bf16[16,48,256]{2,1,0:T(8,128)(2,1)}), bf16[16,48,256]{2,1,0:T(8,128)(2,1)S(1)}, u32[]{:S(2)}, u32[]{:S(2)}) %all-to-all-start.1) | async-done | bytes 393248 | tf_op jit(solution)/shard_map/all_to_all | solution.py:301
  58.6 0.8 %squares.1 = f32[8,1,128]{2,1,0:T(1,128)} custom-call(bf16[16,48,256]{2,1,0:T(8,128)(2,1)S(1)} %all-to-all-done.1.arrived_ref), custom_call_target="tpu_custom_call" | custom-call | tf_op jit(solution)/shard_map/squares/pallas_call | solution.py:106
  59.4 4.5 %all-to-all-start.2 = ((f32[8,1,128]{2,1,0:T(1,128)}), f32[8,1,128]{2,1,0:T(1,128)S(1)}, u32[]{:S(2)}, u32[]{:S(2)}) async-start(f32[8,1,128]{2,1,0:T(1,128)} %squares.1), calls=%async_computation.2 | async-start | bytes 8192 | tf_op jit(solution)/shard_map/all_to_all | solution.py:305
  63.9 5.2 %all-to-all-done.2.sums_ref = f32[8,1,128]{2,1,0:T(1,128)S(1)} async-done(((f32[8,1,128]{2,1,0:T(1,128)}), f32[8,1,128]{2,1,0:T(1,128)S(1)}, u32[]{:S(2)}, u32[]{:S(2)}) %all-to-all-start.2) | async-done | bytes 4128 | tf_op jit(solution)/shard_map/all_to_all | solution.py:305
  69.1 6.0 %finish.1 = (f32[128,256]{1,0:T(8,128)}, f32[128,256]{1,0:T(8,128)}, f32[256,128]{1,0:T(8,128)}, bf16[2048,256]{1,0:T(8,128)(2,1)}, bf16[2048,256]{1,0:T(8,128)(...) custom-call(s32[1]{0:T(128)} %bitcast.me_ref, ...), custom_call_target="tpu_custom_call" | custom-call | tf_op jit(solution)/shard_map/finish/pallas_call | solution.py:209
  (23 shorter events, 0.0 us)
Async XLA Ops:
  0.6 10.0 %copy-start = (bf16[2048,256]{1,0:T(8,128)(2,1)S(1)}, bf16[2048,256]{1,0:T(8,128)(2,1)}, u32[]{:S(2)}) copy-start(bf16[2048,256]{1,0:T(8,128)(2,1)} %param.12) | copy-start | bytes 3145732
  0.7 1.0 %copy-start.3 = (f32[256,128]{1,0:T(8,128)S(1)}, f32[256,128]{1,0:T(8,128)}, u32[]{:S(2)}) copy-start(f32[256,128]{1,0:T(8,128)} %outw_ref.1) | copy-start | bytes 393220
  0.7 1.0 %copy-start.2 = (f32[128,256]{1,0:T(8,128)S(1)}, f32[128,256]{1,0:T(8,128)}, u32[]{:S(2)}) copy-start(f32[128,256]{1,0:T(8,128)} %value_ref.3) | copy-start | bytes 393220
  0.7 1.1 %copy-start.1 = (f32[128,256]{1,0:T(8,128)S(1)}, f32[128,256]{1,0:T(8,128)}, u32[]{:S(2)}) copy-start(f32[128,256]{1,0:T(8,128)} %forget_ref.3) | copy-start | bytes 393220
  0.7 7.6 %slice-start = ((s8[8388608]{0:T(1024)(128)(4,1)}), s8[4194304]{0:T(1024)(128)(4,1)S(1)}, s32[]{:S(2)}) async-start(s8[8388608]{0:T(1024)(128)(4,1)} %bitcast.35), calls=%async_computation.3 | async-start | bytes 8388608
  1.8 6.5 %copy-start.6 = (bf16[3,2048,256]{2,1,0:T(8,128)(2,1)S(1)}, bf16[3,2048,256]{2,1,0:T(8,128)(2,1)}, u32[]{:S(2)}) copy-start(bf16[3,2048,256]{2,1,0:T(8,128)(2,1)} %mine_ref.1) | copy-start | bytes 9437188
  1.8 6.5 %slice-start.1 = ((s8[8388608]{0:T(1024)(128)(4,1)}), s8[4194304]{0:T(1024)(128)(4,1)S(1)}, s32[]{:S(2)}) async-start(s8[8388608]{0:T(1024)(128)(4,1)} %bitcast.35), calls=%async_computation.4 | async-start | bytes 8388608
  2.5 15.7 %collective-permute-start.2 = (bf16[1,384,256]{2,1,0:T(8,128)(2,1)}, bf16[1,384,256]{2,1,0:T(8,128)(2,1)S(1)}, u32[]{:S(2)}, u32[]{:S(2)}) collective-permute-start(bf16[1,384,256]{2,1,0:T(8,128)(2,1)} %pack.1.own_ref), channel_id=1, source_target_pairs={{0,8},{8,16},{16,24},{24,0},{32,40},{40,48},{48,56},{56,32},{64,72... | collective-permute-start | bytes 589832 | tf_op jit(solution)/shard_map/ppermute | solution.py:243
  4.1 14.1 %collective-permute-start.1 = (bf16[1,384,256]{2,1,0:T(8,128)(2,1)}, bf16[1,384,256]{2,1,0:T(8,128)(2,1)S(1)}, u32[]{:S(2)}, u32[]{:S(2)}) collective-permute-start(bf16[1,384,256]{2,1,0:T(8,128)(2,1)} %pack.1.own_ref), channel_id=1, source_target_pairs={{0,16},{8,24},{16,0},{24,8},{32,48},{40,56},{48,32},{56,40},{64,80... | collective-permute-start | bytes 589832 | tf_op jit(solution)/shard_map/ppermute | solution.py:243
  6.8 11.3 %collective-permute-start = (bf16[1,384,256]{2,1,0:T(8,128)(2,1)}, bf16[1,384,256]{2,1,0:T(8,128)(2,1)S(1)}, u32[]{:S(2)}, u32[]{:S(2)}) collective-permute-start(bf16[1,384,256]{2,1,0:T(8,128)(2,1)} %pack.1.own_ref), channel_id=1, source_target_pairs={{0,24},{8,0},{16,8},{24,16},{32,56},{40,32},{48,40},{56,48},{64,88... | collective-permute-start | bytes 589832 | tf_op jit(solution)/shard_map/ppermute | solution.py:243
  10.7 3.3 %slice-start.2 = ((s8[8388608]{0:T(1024)(128)(4,1)}), s8[4194304]{0:T(1024)(128)(4,1)S(1)}, s32[]{:S(2)}) async-start(s8[8388608]{0:T(1024)(128)(4,1)} %bitcast.37), calls=%async_computation.5 | async-start | bytes 8388608
  11.1 2.4 %copy-start.7 = (bf16[2048,256]{1,0:T(8,128)(2,1)S(1)}, bf16[2048,256]{1,0:T(8,128)(2,1)}, u32[]{:S(2)}) copy-start(bf16[2048,256]{1,0:T(8,128)(2,1)} %param.13) | copy-start | bytes 3145732
  11.1 3.4 %slice-start.3 = ((s8[8388608]{0:T(1024)(128)(4,1)}), s8[4194304]{0:T(1024)(128)(4,1)S(1)}, s32[]{:S(2)}) async-start(s8[8388608]{0:T(1024)(128)(4,1)} %bitcast.37), calls=%async_computation.6 | async-start | bytes 8388608
  14.5 2.4 %copy-start.8 = (bf16[2048,256]{1,0:T(8,128)(2,1)S(1)}, bf16[2048,256]{1,0:T(8,128)(2,1)}, u32[]{:S(2)}) copy-start(bf16[2048,256]{1,0:T(8,128)(2,1)} %param.14) | copy-start | bytes 3145732
  14.5 27.9 %copy-start.4 = (f32[16,3,256]{2,0,1:T(8,128)S(1)}, f32[16,3,256]{2,0,1:T(8,128)}, u32[]{:S(2)}) copy-start(f32[16,3,256]{2,0,1:T(8,128)} %param.20) | copy-start | bytes 147460
  14.5 27.9 %copy-start.5 = (f32[16,3,256]{2,0,1:T(8,128)S(1)}, f32[16,3,256]{2,0,1:T(8,128)}, u32[]{:S(2)}) copy-start(f32[16,3,256]{2,0,1:T(8,128)} %param.21) | copy-start | bytes 147460
  19.1 19.4 %collective-permute-start.3 = (bf16[2,384,256]{2,1,0:T(8,128)(2,1)S(1)}, bf16[2,384,256]{2,1,0:T(8,128)(2,1)S(1)}, u32[]{:S(2)}, u32[]{:S(2)}) collective-permute-start(bf16[2,384,256]{2,1,0:T(8,128)(2,1)S(1)} %get-tuple-element.42.refs_0_), channel_id=1, source_target_pairs={{0,32},{8,40},{16,48},{24,56},{32,0},{40,8},{48,16},{56,24},{64,96... | collective-permute-start | bytes 1179656 | tf_op jit(solution)/shard_map/ppermute | solution.py:247
  21.1 21.3 %collective-permute-start.7 = (bf16[2,384,256]{2,1,0:T(8,128)(2,1)S(1)}, bf16[2,384,256]{2,1,0:T(8,128)(2,1)S(1)}, u32[]{:S(2)}, u32[]{:S(2)}) collective-permute-start(bf16[2,384,256]{2,1,0:T(8,128)(2,1)S(1)} %get-tuple-element.43.refs_5_), channel_id=1, source_target_pairs={{0,96},{8,104},{16,112},{24,120},{32,64},{40,72},{48,80},{56,88},{... | collective-permute-start | bytes 1179656 | tf_op jit(solution)/shard_map/ppermute | solution.py:247
  23.7 18.7 %all-to-all-start = ((bf16[16,3,16,256]{3,2,1,0:T(8,128)(2,1)}), bf16[16,3,16,256]{3,2,1,0:T(8,128)(2,1)S(1)}, u32[]{:S(2)}, u32[]{:S(2)}) async-start(bf16[16,3,16,256]{3,2,1,0:T(8,128)(2,1)} %pad_maximum_fusion), calls=%async_computation | async-start | bytes 786432 | tf_op jit(solution)/shard_map/all_to_all | solution.py:295
  27.2 10.7 %collective-permute-start.8 = (bf16[1,384,256]{2,1,0:T(8,128)(2,1)}, bf16[1,384,256]{2,1,0:T(8,128)(2,1)}, u32[]{:S(2)}, u32[]{:S(2)}) collective-permute-start(bf16[1,384,256]{2,1,0:T(8,128)(2,1)} %pack.1.own_ref), channel_id=1, source_target_pairs={{0,32},{8,40},{16,48},{24,56},{32,0},{40,8},{48,16},{56,24},{64,96... | collective-permute-start | bytes 589832 | tf_op jit(solution)/shard_map/ppermute | solution.py:247
  29.1 19.7 %collective-permute-start.4 = (bf16[1,384,256]{2,1,0:T(8,128)(2,1)}, bf16[1,384,256]{2,1,0:T(8,128)(2,1)}, u32[]{:S(2)}, u32[]{:S(2)}) collective-permute-start(bf16[1,384,256]{2,1,0:T(8,128)(2,1)} %pack.1.own_ref), channel_id=1, source_target_pairs={{0,96},{8,104},{16,112},{24,120},{32,64},{40,72},{48,80},{56,88},{... | collective-permute-start | bytes 589832 | tf_op jit(solution)/shard_map/ppermute | solution.py:247
  37.9 14.0 %collective-permute-start.9 = (bf16[1,384,256]{2,1,0:T(8,128)(2,1)}, bf16[1,384,256]{2,1,0:T(8,128)(2,1)}, u32[]{:S(2)}, u32[]{:S(2)}) collective-permute-start(bf16[1,384,256]{2,1,0:T(8,128)(2,1)} %collective-permute-done.8), channel_id=1, source_target_pairs={{0,8},{8,16},{16,24},{24,0},{32,40},{40,48},{48,56},{56,32},{64,72... | collective-permute-start | bytes 589832 | tf_op jit(solution)/shard_map/ppermute | solution.py:243
  38.5 30.6 %collective-permute-start.6 = (bf16[2,384,256]{2,1,0:T(8,128)(2,1)S(1)}, bf16[2,384,256]{2,1,0:T(8,128)(2,1)S(1)}, u32[]{:S(2)}, u32[]{:S(2)}) collective-permute-start(bf16[2,384,256]{2,1,0:T(8,128)(2,1)S(1)} %collective-permute-done.3.refs_1_), channel_id=1, source_target_pairs={{0,96},{8,104},{16,112},{24,120},{32,64},{40,72},{48,80},{56,88},{... | collective-permute-start | bytes 1179656 | tf_op jit(solution)/shard_map/ppermute | solution.py:247
  42.4 26.7 %collective-permute-start.11 = (bf16[2,384,256]{2,1,0:T(8,128)(2,1)S(1)}, bf16[2,384,256]{2,1,0:T(8,128)(2,1)}, u32[]{:S(2)}, u32[]{:S(2)}) collective-permute-start(bf16[2,384,256]{2,1,0:T(8,128)(2,1)S(1)} %collective-permute-done.7.refs_6_), channel_id=1, source_target_pairs={{0,32},{8,40},{16,48},{24,56},{32,0},{40,8},{48,16},{56,24},{64,96... | collective-permute-start | bytes 1179656 | tf_op jit(solution)/shard_map/ppermute | solution.py:247
  43.3 15.3 %all-to-all-start.1 = ((bf16[16,48,256]{2,1,0:T(8,128)(2,1)}), bf16[16,48,256]{2,1,0:T(8,128)(2,1)S(1)}, u32[]{:S(2)}, u32[]{:S(2)}) async-start(bf16[16,48,256]{2,1,0:T(8,128)(2,1)} %get-tuple-element.41), calls=%async_computation.1 | async-start | bytes 786432 | tf_op jit(solution)/shard_map/all_to_all | solution.py:301
  48.8 15.1 %collective-permute-start.5 = (bf16[1,384,256]{2,1,0:T(8,128)(2,1)}, bf16[1,384,256]{2,1,0:T(8,128)(2,1)}, u32[]{:S(2)}, u32[]{:S(2)}) collective-permute-start(bf16[1,384,256]{2,1,0:T(8,128)(2,1)} %collective-permute-done.4.refs_2_), channel_id=1, source_target_pairs={{0,24},{8,0},{16,8},{24,16},{32,56},{40,32},{48,40},{56,48},{64,88... | collective-permute-start | bytes 589832 | tf_op jit(solution)/shard_map/ppermute | solution.py:243
  52.0 11.9 %collective-permute-start.10 = (bf16[1,384,256]{2,1,0:T(8,128)(2,1)}, bf16[1,384,256]{2,1,0:T(8,128)(2,1)}, u32[]{:S(2)}, u32[]{:S(2)}) collective-permute-start(bf16[1,384,256]{2,1,0:T(8,128)(2,1)} %collective-permute-done.9.refs_8_), channel_id=1, source_target_pairs={{0,8},{8,16},{16,24},{24,0},{32,40},{40,48},{48,56},{56,32},{64,72... | collective-permute-start | bytes 589832 | tf_op jit(solution)/shard_map/ppermute | solution.py:243
  59.4 9.7 %all-to-all-start.2 = ((f32[8,1,128]{2,1,0:T(1,128)}), f32[8,1,128]{2,1,0:T(1,128)S(1)}, u32[]{:S(2)}, u32[]{:S(2)}) async-start(f32[8,1,128]{2,1,0:T(1,128)} %squares.1), calls=%async_computation.2 | async-start | bytes 8192 | tf_op jit(solution)/shard_map/all_to_all | solution.py:305

commit v4 on v3

--- a/solution.py
+++ b/solution.py
@@ -166,24 +166,20 @@
     full = lax.dot_general(dir_ref[2], base_ref[2], by_columns, preferred_element_type=jnp.float32)
     moves.append(full * (0.01 * scale_ref[0, 2]))
     blocks = base_ref.shape[1] // block
+    rows_here = blocks // SIDE
+    for j in range(rows_here):
+        away = (step * rows_here + j) ^ (me // SIDE)
+        for t, (near, far) in enumerate(TURNS):
+            for sources, mask in zip(held[t], (0, near, far, near ^ far)):
+
+                @pl.when(away == mask)
+                def _(sources=sources, t=t, j=j):
+                    for n in range(2):
+                        owner = j * SIDE + (me + 2 * t + n) % SIDE
+                        old_ref[owner] = sources[n][0] if isinstance(sources, tuple) else sources[n]
+
     for j in range(blocks):
-        owner = step * blocks + j
-        place = (owner - me) % SIDE
-        away = owner // SIDE ^ me // SIDE
-        for t, (near, far) in enumerate(TURNS):
-
-            @pl.when(place // 2 == t)
-            def _(t=t, near=near, far=far):
-                for sources, mask in zip(held[t], (0, near, far, near ^ far)):
-
-                    @pl.when(away == mask)
-                    def _(sources=sources):
-                        if isinstance(sources, tuple):
-                            old_ref[...] = jnp.where(place % 2 == 0, sources[0][0], sources[1][0])
-                        else:
-                            old_ref[...] = sources[place % 2]
-
-        old = old_ref[...].astype(jnp.float32)
+        old = old_ref[j].astype(jnp.float32)
         near = slice(j * block, (j + 1) * block)
         copy_forget[near] = (old[:block] - moves[0][near]).astype(jnp.bfloat16)
         copy_value[near] = (old[block : 2 * block] - moves[1][near]).astype(jnp.bfloat16)
@@ -229,7 +225,7 @@
             scratch_shapes=[
                 pltpu.VMEM((3, rank, columns), jnp.bfloat16),
                 pltpu.VMEM((1, 128), jnp.float32),
-                pltpu.VMEM(flat[0].shape[1:], flat[0].dtype),
+                pltpu.VMEM((tile // block, *flat[0].shape[1:]), flat[0].dtype),
             ],
         ),
         out_shape=(*own, *copies, *own),
@@ -294,13 +290,13 @@
     part, *held = lax.optimization_barrier((part, *held))
     arrived = lax.all_to_all(part, FS, split_axis=0, concat_axis=0, tiled=True)
     nearer = [passed(a, near) for a, (near, _) in zip(held, TURNS)]
-    far_one, near_three = along(at_far, 1), along(at_near, 3)
     moment_one, moment_two, messages = moments(
         arrived, jnp.moveaxis(first_moment, 1, 0), jnp.moveaxis(second_moment, 1, 0)
     )
     gathered = lax.all_to_all(messages, FS, split_axis=0, concat_axis=0, tiled=True)
+    far_one = along(at_far, 1)
+    near_two, near_three = along(at_near, 2), along(at_near, 3)
     across = [passed(a, far) for a, (_, far) in zip(nearer, TURNS)]
-    near_two = along(near_three, 3)
     sums = squares(gathered, lax.axis_size(TP))
     sums = lax.all_to_all(sums, TP, split_axis=0, concat_axis=0, tiled=True)
     entries = float(rank * columns * lax.axis_size(TP))

time: 76.2 us -> 72.2 us (0.948)
  waiting for transfers between devices: 18.6 us -> 12.6 us
  starting transfers between devices: 35.4 us -> 37.9 us
    ppermute x6, waiting for transfers between devices: 6.81 us -> 2.27 us  [passed(): lax.ppermute(value, FS, [(i, i ^ mask * SIDE) for i in range(lax.axis_siz...]
    ppermute x6, starting transfers between devices: 9.57 us -> 11.9 us  [along(): return lax.ppermute(value, FS, pairs)]
    all_to_all x1, waiting for transfers between devices: 6.61 us -> 4.65 us  [on_device(): lax.all_to_all(messages, FS, split_axis=0, concat_axis=0, tiled=True)]
    ppermute x6, starting transfers between devices: 12.3 us -> 13.4 us  [passed(): lax.ppermute(value, FS, [(i, i ^ mask * SIDE) for i in range(lax.axis_siz...]
    all_to_all x1, starting transfers between devices: 5.47 us -> 4.52 us  [on_device(): lax.all_to_all(messages, FS, split_axis=0, concat_axis=0, tiled=True)]
  transfers between devices with their start and end apart: 15 -> 15, of which waited for: 3 -> 4; matrix products, arithmetic and copies ran while one was open for 12% -> 13% of each run, Pallas kernels for 2% -> 2%
where the time goes in v4:
time: 72.2 us; the launch traced here: 71.1 us
  starting transfers between devices  37.9 us (52%)
  waiting for transfers between devices  12.6 us (17%)
  Pallas kernels  8.81 us (12%)
  matrix products  8.49 us (12%)
  local copies, waits for them, and re-layouts  1.6 us (2%)
  between operations  0.92 us (1%)
  other arithmetic  0.79 us (1%)
    ppermute x6, starting transfers between devices, passed(): lax.ppermute(value, FS, [(i, i ^ mask * SIDE) for i in range(lax.axis_siz...  13.4 us
    ppermute x6, starting transfers between devices, along(): return lax.ppermute(value, FS, pairs)  11.9 us
    dot_general x3, matrix products, reduced_part(): lax.dot_general(basis, x, (((0,), (1,)), ((), ())), preferred_element_typ...  7.08 us
    pallas_call x1, Pallas kernels, finish(): pl.pallas_call(functools.partial(finish_kernel, entries), grid_spec=pltpu...  5.45 us
    all_to_all x1, waiting for transfers between devices, on_device(): sums = lax.all_to_all(sums, TP, split_axis=0, concat_axis=0, tiled=True)  5.19 us
    all_to_all x1, waiting for transfers between devices, on_device(): lax.all_to_all(messages, FS, split_axis=0, concat_axis=0, tiled=True)  4.65 us
    all_to_all x1, starting transfers between devices, on_device(): lax.all_to_all(messages, FS, split_axis=0, concat_axis=0, tiled=True)  4.52 us
    all_to_all x1, starting transfers between devices, on_device(): sums = lax.all_to_all(sums, TP, split_axis=0, concat_axis=0, tiled=True)  4.48 us
  transfers between devices with their start and end apart: 15, of which 4 were waited for; matrix products, arithmetic and copies ran while one was open for 13% of the time, Pallas kernels for 2%

profile of v4, /device:TPU:0, one launch (start us, length us, event | category | flops | bytes accessed | tf_op | source)
XLA Modules:
  0.0 71.1 jit_solution(3063744311796021157)
XLA Ops:
  0.6 0.0 copy-start
  0.7 0.0 copy-start.3
  0.7 0.0 copy-start.2
  0.7 0.0 copy-start.1
  0.7 0.0 slice-start
  0.7 0.9 %copy-done.3 = f32[256,128]{1,0:T(8,128)S(1)} copy-done((f32[256,128]{1,0:T(8,128)S(1)}, f32[256,128]{1,0:T(8,128)}, u32[]{:S(2)}) %copy-start.3) | copy-done | bytes 131096
  1.7 0.1 copy-done.2
  1.7 0.1 copy-done.1
  1.8 0.7 pack.1.own_ref
  2.5 1.6 %collective-permute-start.2 = (bf16[1,384,256]{2,1,0:T(8,128)(2,1)}, bf16[1,384,256]{2,1,0:T(8,128)(2,1)S(1)}, u32[]{:S(2)}, u32[]{:S(2)}) collective-permute-start(bf16[1,384,256]{2,1,0:T(8,128)(2,1)} %pack.1.own_ref), channel_id=1, source_target_pairs={{0,8},{8,16},{16,24},{24,0},{32,40},{40,48},{48,56},{56,32},{64,72... | collective-permute-start | bytes 589832 | tf_op jit(solution)/shard_map/ppermute | solution.py:239
  4.1 2.7 %collective-permute-start.1 = (bf16[1,384,256]{2,1,0:T(8,128)(2,1)}, bf16[1,384,256]{2,1,0:T(8,128)(2,1)S(1)}, u32[]{:S(2)}, u32[]{:S(2)}) collective-permute-start(bf16[1,384,256]{2,1,0:T(8,128)(2,1)} %pack.1.own_ref), channel_id=1, source_target_pairs={{0,16},{8,24},{16,0},{24,8},{32,48},{40,56},{48,32},{56,40},{64,80... | collective-permute-start | bytes 589832 | tf_op jit(solution)/shard_map/ppermute | solution.py:239
  6.8 1.4 %collective-permute-start = (bf16[1,384,256]{2,1,0:T(8,128)(2,1)}, bf16[1,384,256]{2,1,0:T(8,128)(2,1)S(1)}, u32[]{:S(2)}, u32[]{:S(2)}) collective-permute-start(bf16[1,384,256]{2,1,0:T(8,128)(2,1)} %pack.1.own_ref), channel_id=1, source_target_pairs={{0,24},{8,0},{16,8},{24,16},{32,56},{40,32},{48,40},{56,48},{64,88... | collective-permute-start | bytes 589832 | tf_op jit(solution)/shard_map/ppermute | solution.py:239
  8.3 2.4 %convolution_convert_fusion.2 = bf16[256,2048]{1,0:T(8,128)(2,1)S(1)} fusion(bf16[2048,2048]{1,0:T(8,128)(2,1)S(1)} %bitcast.36, bf16[3,2048,256]{2,1,0:T(8,128)(2,1)S(1)} %copy-done.6), kind=kOutput, calls=%fused_computation.2 | convolution fusion | flops 2148007936 | bytes 10485760 | tf_op jit(solution)/shard_map/dot_general | solution.py:59
  10.7 0.0 slice-start.2
  10.7 0.4 fusion.2
  11.1 0.0 copy-start.7
  11.1 0.0 slice-start.3
  11.2 2.3 %fusion = bf16[256,2048]{0,1:T(8,128)(2,1)S(1)} fusion(bf16[2048,2048]{1,0:T(8,128)(2,1)S(1)} %bitcast.36, bf16[3,2048,256]{2,1,0:T(8,128)(2,1)S(1)} %copy-done.6), kind=kOutput, calls=%fused_computation.3 | convolution fusion | flops 2148007936 | bytes 10485760 | tf_op jit(solution)/shard_map/dot_general | solution.py:59
  13.5 0.5 fusion.3
  14.0 0.5 slice-done.3
  14.5 2.3 %fusion.1 = bf16[256,2048]{0,1:T(8,128)(2,1)S(1)} fusion(bf16[2048,2048]{1,0:T(8,128)(2,1)S(1)} %bitcast.38, bf16[3,2048,256]{2,1,0:T(8,128)(2,1)S(1)} %copy-done.6), kind=kOutput, calls=%fused_computation.4 | convolution fusion | flops 2148007936 | bytes 10485760 | tf_op jit(solution)/shard_map/dot_general | solution.py:59
  16.9 0.5 fusion.4
  17.4 0.8 %pad_maximum_fusion = bf16[16,3,16,256]{3,2,1,0:T(8,128)(2,1)} fusion(bf16[16,1,16,256]{3,2,1,0:T(8,128)(2,1)S(1)} %bitcast.33, bf16[16,1,16,256]{3,2,1,0:T(8,128)(2,1)S(1)} %bitcast.32, bf16[16,1,16,256]{3,2,1,0:T(8,128)(2,1)S(1)} %bitcast.34), kind=kLoop, calls=%fused_computation.17 | loop fusion | flops 393216 | bytes 786432 | tf_op jit(solution)/shard_map/stack | solution.py:288
  18.1 0.0 collective-permute-done.2.three_ref
  18.1 0.0 collective-permute-done.1.two_ref
  18.2 0.0 collective-permute-done.one_ref
  18.2 1.0 %join.1 = (bf16[2,384,256]{2,1,0:T(8,128)(2,1)S(1)}, bf16[2,384,256]{2,1,0:T(8,128)(2,1)S(1)}) custom-call(bf16[1,384,256]{2,1,0:T(8,128)(2,1)} %pack.1.own_ref, bf16[1,384,256]{2,1,0:T(8,128)(2,1)S(1)} %collective-permute-done.one_ref, bf16[1,384,256]{2,1,0:T(8,128)(2,1)S(1)} %collective-permute-done.1.two_ref, ...), custom_call_target="tpu_custom_call" | custom-call | tf_op jit(solution)/shard_map/join/pallas_call | solution.py:256
  19.1 2.0 %collective-permute-start.3 = (bf16[2,384,256]{2,1,0:T(8,128)(2,1)S(1)}, bf16[2,384,256]{2,1,0:T(8,128)(2,1)S(1)}, u32[]{:S(2)}, u32[]{:S(2)}) collective-permute-start(bf16[2,384,256]{2,1,0:T(8,128)(2,1)S(1)} %get-tuple-element.42.refs_0_), channel_id=1, source_target_pairs={{0,32},{8,40},{16,48},{24,56},{32,0},{40,8},{48,16},{56,24},{64,96... | collective-permute-start | bytes 1179656 | tf_op jit(solution)/shard_map/ppermute | solution.py:243
  21.1 2.5 %collective-permute-start.7 = (bf16[2,384,256]{2,1,0:T(8,128)(2,1)S(1)}, bf16[2,384,256]{2,1,0:T(8,128)(2,1)S(1)}, u32[]{:S(2)}, u32[]{:S(2)}) collective-permute-start(bf16[2,384,256]{2,1,0:T(8,128)(2,1)S(1)} %get-tuple-element.43.refs_5_), channel_id=1, source_target_pairs={{0,96},{8,104},{16,112},{24,120},{32,64},{40,72},{48,80},{56,88},{... | collective-permute-start | bytes 1179656 | tf_op jit(solution)/shard_map/ppermute | solution.py:243
  23.7 3.6 %all-to-all-start = ((bf16[16,3,16,256]{3,2,1,0:T(8,128)(2,1)}), bf16[16,3,16,256]{3,2,1,0:T(8,128)(2,1)S(1)}, u32[]{:S(2)}, u32[]{:S(2)}) async-start(bf16[16,3,16,256]{3,2,1,0:T(8,128)(2,1)} %pad_maximum_fusion), calls=%async_computation | async-start | bytes 786432 | tf_op jit(solution)/shard_map/all_to_all | solution.py:291
  27.2 1.8 %collective-permute-start.8 = (bf16[1,384,256]{2,1,0:T(8,128)(2,1)}, bf16[1,384,256]{2,1,0:T(8,128)(2,1)}, u32[]{:S(2)}, u32[]{:S(2)}) collective-permute-start(bf16[1,384,256]{2,1,0:T(8,128)(2,1)} %pack.1.own_ref), channel_id=1, source_target_pairs={{0,32},{8,40},{16,48},{24,56},{32,0},{40,8},{48,16},{56,24},{64,96... | collective-permute-start | bytes 589832 | tf_op jit(solution)/shard_map/ppermute | solution.py:243
  29.1 2.1 %collective-permute-start.4 = (bf16[1,384,256]{2,1,0:T(8,128)(2,1)}, bf16[1,384,256]{2,1,0:T(8,128)(2,1)}, u32[]{:S(2)}, u32[]{:S(2)}) collective-permute-start(bf16[1,384,256]{2,1,0:T(8,128)(2,1)} %pack.1.own_ref), channel_id=1, source_target_pairs={{0,96},{8,104},{16,112},{24,120},{32,64},{40,72},{48,80},{56,88},{... | collective-permute-start | bytes 589832 | tf_op jit(solution)/shard_map/ppermute | solution.py:243
  31.1 2.3 %collective-permute-done.3.refs_1_ = bf16[2,384,256]{2,1,0:T(8,128)(2,1)S(1)} collective-permute-done((bf16[2,384,256]{2,1,0:T(8,128)(2,1)S(1)}, bf16[2,384,256]{2,1,0:T(8,128)(2,1)S(1)}, u32[]{:S(2)}, u32[]{:S(2)}) %collective-permute-start.3) | collective-permute-done | bytes 393248 | tf_op jit(solution)/shard_map/ppermute | solution.py:243
  33.4 5.0 %collective-permute-start.6 = (bf16[2,384,256]{2,1,0:T(8,128)(2,1)S(1)}, bf16[2,384,256]{2,1,0:T(8,128)(2,1)S(1)}, u32[]{:S(2)}, u32[]{:S(2)}) collective-permute-start(bf16[2,384,256]{2,1,0:T(8,128)(2,1)S(1)} %collective-permute-done.3.refs_1_), channel_id=1, source_target_pairs={{0,96},{8,104},{16,112},{24,120},{32,64},{40,72},{48,80},{56,88},{... | collective-permute-start | bytes 1179656 | tf_op jit(solution)/shard_map/ppermute | solution.py:243
  38.4 0.0 collective-permute-start.11
  38.4 0.5 all-to-all-done.arrived_ref
  38.9 0.9 %moments.1 = (f32[3,16,256]{2,1,0:T(8,128)}, f32[3,16,256]{2,1,0:T(8,128)}, bf16[16,48,256]{2,1,0:T(8,128)(2,1)}) custom-call(bf16[16,3,16,256]{3,2,1,0:T(8,128)(2,1)S(1)} %all-to-all-done.arrived_ref, f32[3,16,256]{2,1,0:T(8,128)S(1)} %bitcast.30, f32[3,16,256]{2,1,0:T(8,128)S(1)} %bitcast.31), custom_call_target="tpu_custom_call" | custom-call | tf_op jit(solution)/shard_map/moments/pallas_call | solution.py:87
  39.8 4.5 %all-to-all-start.1 = ((bf16[16,48,256]{2,1,0:T(8,128)(2,1)}), bf16[16,48,256]{2,1,0:T(8,128)(2,1)S(1)}, u32[]{:S(2)}, u32[]{:S(2)}) async-start(bf16[16,48,256]{2,1,0:T(8,128)(2,1)} %get-tuple-element.41), calls=%async_computation.1 | async-start | bytes 786432 | tf_op jit(solution)/shard_map/all_to_all | solution.py:296
  44.3 2.0 %collective-permute-start.10 = (bf16[1,384,256]{2,1,0:T(8,128)(2,1)}, bf16[1,384,256]{2,1,0:T(8,128)(2,1)}, u32[]{:S(2)}, u32[]{:S(2)}) collective-permute-start(bf16[1,384,256]{2,1,0:T(8,128)(2,1)} %collective-permute-done.8), channel_id=1, source_target_pairs={{0,8},{8,16},{16,24},{24,0},{32,40},{40,48},{48,56},{56,32},{64,72... | collective-permute-start | bytes 589832 | tf_op jit(solution)/shard_map/ppermute | solution.py:239
  46.3 2.7 %collective-permute-start.9 = (bf16[1,384,256]{2,1,0:T(8,128)(2,1)}, bf16[1,384,256]{2,1,0:T(8,128)(2,1)}, u32[]{:S(2)}, u32[]{:S(2)}) collective-permute-start(bf16[1,384,256]{2,1,0:T(8,128)(2,1)} %collective-permute-done.8), channel_id=1, source_target_pairs={{0,16},{8,24},{16,0},{24,8},{32,48},{40,56},{48,32},{56,40},{64,80... | collective-permute-start | bytes 589832 | tf_op jit(solution)/shard_map/ppermute | solution.py:239
  49.0 1.5 %collective-permute-start.5 = (bf16[1,384,256]{2,1,0:T(8,128)(2,1)}, bf16[1,384,256]{2,1,0:T(8,128)(2,1)}, u32[]{:S(2)}, u32[]{:S(2)}) collective-permute-start(bf16[1,384,256]{2,1,0:T(8,128)(2,1)} %collective-permute-done.4.refs_2_), channel_id=1, source_target_pairs={{0,24},{8,0},{16,8},{24,16},{32,56},{40,32},{48,40},{56,48},{64,88... | collective-permute-start | bytes 589832 | tf_op jit(solution)/shard_map/ppermute | solution.py:239
  50.4 4.6 %all-to-all-done.1.arrived_ref = bf16[16,48,256]{2,1,0:T(8,128)(2,1)S(1)} async-done(((bf16[16,48,256]{2,1,0:T(8,128)(2,1)}), bf16[16,48,256]{2,1,0:T(8,128)(2,1)S(1)}, u32[]{:S(2)}, u32[]{:S(2)}) %all-to-all-start.1) | async-done | bytes 393248 | tf_op jit(solution)/shard_map/all_to_all | solution.py:296
  55.1 0.8 %squares.1 = f32[8,1,128]{2,1,0:T(1,128)} custom-call(bf16[16,48,256]{2,1,0:T(8,128)(2,1)S(1)} %all-to-all-done.1.arrived_ref), custom_call_target="tpu_custom_call" | custom-call | tf_op jit(solution)/shard_map/squares/pallas_call | solution.py:106
  55.9 4.5 %all-to-all-start.2 = ((f32[8,1,128]{2,1,0:T(1,128)}), f32[8,1,128]{2,1,0:T(1,128)S(1)}, u32[]{:S(2)}, u32[]{:S(2)}) async-start(f32[8,1,128]{2,1,0:T(1,128)} %squares.1), calls=%async_computation.2 | async-start | bytes 8192 | tf_op jit(solution)/shard_map/all_to_all | solution.py:301
  60.4 0.0 collective-permute-done.10.refs_8_
  60.4 0.0 collective-permute-done.5.refs_3_
  60.4 5.2 %all-to-all-done.2.sums_ref = f32[8,1,128]{2,1,0:T(1,128)S(1)} async-done(((f32[8,1,128]{2,1,0:T(1,128)}), f32[8,1,128]{2,1,0:T(1,128)S(1)}, u32[]{:S(2)}, u32[]{:S(2)}) %all-to-all-start.2) | async-done | bytes 4128 | tf_op jit(solution)/shard_map/all_to_all | solution.py:301
  65.6 5.5 %finish.1 = (f32[128,256]{1,0:T(8,128)}, f32[128,256]{1,0:T(8,128)}, f32[256,128]{1,0:T(8,128)}, bf16[2048,256]{1,0:T(8,128)(2,1)}, bf16[2048,256]{1,0:T(8,128)(...) custom-call(s32[1]{0:T(128)} %bitcast.me_ref, ...), custom_call_target="tpu_custom_call" | custom-call | tf_op jit(solution)/shard_map/finish/pallas_call | solution.py:205
  (23 shorter events, 0.0 us)
Async XLA Ops:
  0.6 10.0 %copy-start = (bf16[2048,256]{1,0:T(8,128)(2,1)S(1)}, bf16[2048,256]{1,0:T(8,128)(2,1)}, u32[]{:S(2)}) copy-start(bf16[2048,256]{1,0:T(8,128)(2,1)} %param.12) | copy-start | bytes 3145732
  0.7 1.0 %copy-start.3 = (f32[256,128]{1,0:T(8,128)S(1)}, f32[256,128]{1,0:T(8,128)}, u32[]{:S(2)}) copy-start(f32[256,128]{1,0:T(8,128)} %outw_ref.1) | copy-start | bytes 393220
  0.7 1.0 %copy-start.2 = (f32[128,256]{1,0:T(8,128)S(1)}, f32[128,256]{1,0:T(8,128)}, u32[]{:S(2)}) copy-start(f32[128,256]{1,0:T(8,128)} %value_ref.3) | copy-start | bytes 393220
  0.7 1.1 %copy-start.1 = (f32[128,256]{1,0:T(8,128)S(1)}, f32[128,256]{1,0:T(8,128)}, u32[]{:S(2)}) copy-start(f32[128,256]{1,0:T(8,128)} %forget_ref.3) | copy-start | bytes 393220
  0.7 7.6 %slice-start = ((s8[8388608]{0:T(1024)(128)(4,1)}), s8[4194304]{0:T(1024)(128)(4,1)S(1)}, s32[]{:S(2)}) async-start(s8[8388608]{0:T(1024)(128)(4,1)} %bitcast.35), calls=%async_computation.3 | async-start | bytes 8388608
  1.8 6.5 %copy-start.6 = (bf16[3,2048,256]{2,1,0:T(8,128)(2,1)S(1)}, bf16[3,2048,256]{2,1,0:T(8,128)(2,1)}, u32[]{:S(2)}) copy-start(bf16[3,2048,256]{2,1,0:T(8,128)(2,1)} %mine_ref.1) | copy-start | bytes 9437188
  1.8 6.5 %slice-start.1 = ((s8[8388608]{0:T(1024)(128)(4,1)}), s8[4194304]{0:T(1024)(128)(4,1)S(1)}, s32[]{:S(2)}) async-start(s8[8388608]{0:T(1024)(128)(4,1)} %bitcast.35), calls=%async_computation.4 | async-start | bytes 8388608
  2.5 15.7 %collective-permute-start.2 = (bf16[1,384,256]{2,1,0:T(8,128)(2,1)}, bf16[1,384,256]{2,1,0:T(8,128)(2,1)S(1)}, u32[]{:S(2)}, u32[]{:S(2)}) collective-permute-start(bf16[1,384,256]{2,1,0:T(8,128)(2,1)} %pack.1.own_ref), channel_id=1, source_target_pairs={{0,8},{8,16},{16,24},{24,0},{32,40},{40,48},{48,56},{56,32},{64,72... | collective-permute-start | bytes 589832 | tf_op jit(solution)/shard_map/ppermute | solution.py:239
  4.1 14.1 %collective-permute-start.1 = (bf16[1,384,256]{2,1,0:T(8,128)(2,1)}, bf16[1,384,256]{2,1,0:T(8,128)(2,1)S(1)}, u32[]{:S(2)}, u32[]{:S(2)}) collective-permute-start(bf16[1,384,256]{2,1,0:T(8,128)(2,1)} %pack.1.own_ref), channel_id=1, source_target_pairs={{0,16},{8,24},{16,0},{24,8},{32,48},{40,56},{48,32},{56,40},{64,80... | collective-permute-start | bytes 589832 | tf_op jit(solution)/shard_map/ppermute | solution.py:239
  6.8 11.3 %collective-permute-start = (bf16[1,384,256]{2,1,0:T(8,128)(2,1)}, bf16[1,384,256]{2,1,0:T(8,128)(2,1)S(1)}, u32[]{:S(2)}, u32[]{:S(2)}) collective-permute-start(bf16[1,384,256]{2,1,0:T(8,128)(2,1)} %pack.1.own_ref), channel_id=1, source_target_pairs={{0,24},{8,0},{16,8},{24,16},{32,56},{40,32},{48,40},{56,48},{64,88... | collective-permute-start | bytes 589832 | tf_op jit(solution)/shard_map/ppermute | solution.py:239
  10.7 3.3 %slice-start.2 = ((s8[8388608]{0:T(1024)(128)(4,1)}), s8[4194304]{0:T(1024)(128)(4,1)S(1)}, s32[]{:S(2)}) async-start(s8[8388608]{0:T(1024)(128)(4,1)} %bitcast.37), calls=%async_computation.5 | async-start | bytes 8388608
  11.1 2.4 %copy-start.7 = (bf16[2048,256]{1,0:T(8,128)(2,1)S(1)}, bf16[2048,256]{1,0:T(8,128)(2,1)}, u32[]{:S(2)}) copy-start(bf16[2048,256]{1,0:T(8,128)(2,1)} %param.13) | copy-start | bytes 3145732
  11.1 3.4 %slice-start.3 = ((s8[8388608]{0:T(1024)(128)(4,1)}), s8[4194304]{0:T(1024)(128)(4,1)S(1)}, s32[]{:S(2)}) async-start(s8[8388608]{0:T(1024)(128)(4,1)} %bitcast.37), calls=%async_computation.6 | async-start | bytes 8388608
  14.5 2.4 %copy-start.8 = (bf16[2048,256]{1,0:T(8,128)(2,1)S(1)}, bf16[2048,256]{1,0:T(8,128)(2,1)}, u32[]{:S(2)}) copy-start(bf16[2048,256]{1,0:T(8,128)(2,1)} %param.14) | copy-start | bytes 3145732
  14.5 24.4 %copy-start.4 = (f32[16,3,256]{2,0,1:T(8,128)S(1)}, f32[16,3,256]{2,0,1:T(8,128)}, u32[]{:S(2)}) copy-start(f32[16,3,256]{2,0,1:T(8,128)} %param.20) | copy-start | bytes 147460
  14.5 24.4 %copy-start.5 = (f32[16,3,256]{2,0,1:T(8,128)S(1)}, f32[16,3,256]{2,0,1:T(8,128)}, u32[]{:S(2)}) copy-start(f32[16,3,256]{2,0,1:T(8,128)} %param.21) | copy-start | bytes 147460
  19.1 14.3 %collective-permute-start.3 = (bf16[2,384,256]{2,1,0:T(8,128)(2,1)S(1)}, bf16[2,384,256]{2,1,0:T(8,128)(2,1)S(1)}, u32[]{:S(2)}, u32[]{:S(2)}) collective-permute-start(bf16[2,384,256]{2,1,0:T(8,128)(2,1)S(1)} %get-tuple-element.42.refs_0_), channel_id=1, source_target_pairs={{0,32},{8,40},{16,48},{24,56},{32,0},{40,8},{48,16},{56,24},{64,96... | collective-permute-start | bytes 1179656 | tf_op jit(solution)/shard_map/ppermute | solution.py:243
  21.1 17.3 %collective-permute-start.7 = (bf16[2,384,256]{2,1,0:T(8,128)(2,1)S(1)}, bf16[2,384,256]{2,1,0:T(8,128)(2,1)S(1)}, u32[]{:S(2)}, u32[]{:S(2)}) collective-permute-start(bf16[2,384,256]{2,1,0:T(8,128)(2,1)S(1)} %get-tuple-element.43.refs_5_), channel_id=1, source_target_pairs={{0,96},{8,104},{16,112},{24,120},{32,64},{40,72},{48,80},{56,88},{... | collective-permute-start | bytes 1179656 | tf_op jit(solution)/shard_map/ppermute | solution.py:243
  23.7 15.2 %all-to-all-start = ((bf16[16,3,16,256]{3,2,1,0:T(8,128)(2,1)}), bf16[16,3,16,256]{3,2,1,0:T(8,128)(2,1)S(1)}, u32[]{:S(2)}, u32[]{:S(2)}) async-start(bf16[16,3,16,256]{3,2,1,0:T(8,128)(2,1)} %pad_maximum_fusion), calls=%async_computation | async-start | bytes 786432 | tf_op jit(solution)/shard_map/all_to_all | solution.py:291
  27.2 17.1 %collective-permute-start.8 = (bf16[1,384,256]{2,1,0:T(8,128)(2,1)}, bf16[1,384,256]{2,1,0:T(8,128)(2,1)}, u32[]{:S(2)}, u32[]{:S(2)}) collective-permute-start(bf16[1,384,256]{2,1,0:T(8,128)(2,1)} %pack.1.own_ref), channel_id=1, source_target_pairs={{0,32},{8,40},{16,48},{24,56},{32,0},{40,8},{48,16},{56,24},{64,96... | collective-permute-start | bytes 589832 | tf_op jit(solution)/shard_map/ppermute | solution.py:243
  29.1 19.9 %collective-permute-start.4 = (bf16[1,384,256]{2,1,0:T(8,128)(2,1)}, bf16[1,384,256]{2,1,0:T(8,128)(2,1)}, u32[]{:S(2)}, u32[]{:S(2)}) collective-permute-start(bf16[1,384,256]{2,1,0:T(8,128)(2,1)} %pack.1.own_ref), channel_id=1, source_target_pairs={{0,96},{8,104},{16,112},{24,120},{32,64},{40,72},{48,80},{56,88},{... | collective-permute-start | bytes 589832 | tf_op jit(solution)/shard_map/ppermute | solution.py:243
  33.4 32.2 %collective-permute-start.6 = (bf16[2,384,256]{2,1,0:T(8,128)(2,1)S(1)}, bf16[2,384,256]{2,1,0:T(8,128)(2,1)S(1)}, u32[]{:S(2)}, u32[]{:S(2)}) collective-permute-start(bf16[2,384,256]{2,1,0:T(8,128)(2,1)S(1)} %collective-permute-done.3.refs_1_), channel_id=1, source_target_pairs={{0,96},{8,104},{16,112},{24,120},{32,64},{40,72},{48,80},{56,88},{... | collective-permute-start | bytes 1179656 | tf_op jit(solution)/shard_map/ppermute | solution.py:243
  38.4 27.2 %collective-permute-start.11 = (bf16[2,384,256]{2,1,0:T(8,128)(2,1)S(1)}, bf16[2,384,256]{2,1,0:T(8,128)(2,1)}, u32[]{:S(2)}, u32[]{:S(2)}) collective-permute-start(bf16[2,384,256]{2,1,0:T(8,128)(2,1)S(1)} %collective-permute-done.7.refs_6_), channel_id=1, source_target_pairs={{0,32},{8,40},{16,48},{24,56},{32,0},{40,8},{48,16},{56,24},{64,96... | collective-permute-start | bytes 1179656 | tf_op jit(solution)/shard_map/ppermute | solution.py:243
  39.8 15.3 %all-to-all-start.1 = ((bf16[16,48,256]{2,1,0:T(8,128)(2,1)}), bf16[16,48,256]{2,1,0:T(8,128)(2,1)S(1)}, u32[]{:S(2)}, u32[]{:S(2)}) async-start(bf16[16,48,256]{2,1,0:T(8,128)(2,1)} %get-tuple-element.41), calls=%async_computation.1 | async-start | bytes 786432 | tf_op jit(solution)/shard_map/all_to_all | solution.py:296
  44.3 16.1 %collective-permute-start.10 = (bf16[1,384,256]{2,1,0:T(8,128)(2,1)}, bf16[1,384,256]{2,1,0:T(8,128)(2,1)}, u32[]{:S(2)}, u32[]{:S(2)}) collective-permute-start(bf16[1,384,256]{2,1,0:T(8,128)(2,1)} %collective-permute-done.8), channel_id=1, source_target_pairs={{0,8},{8,16},{16,24},{24,0},{32,40},{40,48},{48,56},{56,32},{64,72... | collective-permute-start | bytes 589832 | tf_op jit(solution)/shard_map/ppermute | solution.py:239
  46.3 14.1 %collective-permute-start.9 = (bf16[1,384,256]{2,1,0:T(8,128)(2,1)}, bf16[1,384,256]{2,1,0:T(8,128)(2,1)}, u32[]{:S(2)}, u32[]{:S(2)}) collective-permute-start(bf16[1,384,256]{2,1,0:T(8,128)(2,1)} %collective-permute-done.8), channel_id=1, source_target_pairs={{0,16},{8,24},{16,0},{24,8},{32,48},{40,56},{48,32},{56,40},{64,80... | collective-permute-start | bytes 589832 | tf_op jit(solution)/shard_map/ppermute | solution.py:239
  49.0 11.4 %collective-permute-start.5 = (bf16[1,384,256]{2,1,0:T(8,128)(2,1)}, bf16[1,384,256]{2,1,0:T(8,128)(2,1)}, u32[]{:S(2)}, u32[]{:S(2)}) collective-permute-start(bf16[1,384,256]{2,1,0:T(8,128)(2,1)} %collective-permute-done.4.refs_2_), channel_id=1, source_target_pairs={{0,24},{8,0},{16,8},{24,16},{32,56},{40,32},{48,40},{56,48},{64,88... | collective-permute-start | bytes 589832 | tf_op jit(solution)/shard_map/ppermute | solution.py:239
  55.9 9.7 %all-to-all-start.2 = ((f32[8,1,128]{2,1,0:T(1,128)}), f32[8,1,128]{2,1,0:T(1,128)S(1)}, u32[]{:S(2)}, u32[]{:S(2)}) async-start(f32[8,1,128]{2,1,0:T(1,128)} %squares.1), calls=%async_computation.2 | async-start | bytes 8192 | tf_op jit(solution)/shard_map/all_to_all | solution.py:301
